TPU v7x, 32 devices: a whole 2x2x4 slice. The times are simulated.
32 devices in a mesh: ep: 8 (over z, x), tp: 4 (over y, core).
Axes of the slice: x: 2, y: 2, z: 4, core: 2. Of those that a mesh axis runs over, the one named last changes fastest.
Arguments:
- tokens: bfloat16 [4096, 2048], P(('ep', 'tp')), may hold values from -6 to 6
- routes: int32 [4096, 2], P(('ep', 'tp')), may hold values from 0 to 31, as said below
- gates: float32 [4096, 2], P(('ep', 'tp')), may hold values from 0.1 to 0.6
- w_gate: bfloat16 [32, 2048, 768], P(('ep', 'tp')), may hold values from -0.125 to 0.125
- w_up: bfloat16 [32, 2048, 768], P(('ep', 'tp')), may hold values from -0.125 to 0.125
- w_down: bfloat16 [32, 768, 2048], P(('ep', 'tp')), may hold values from -0.21875 to 0.21875
- moe_out: bfloat16 [4096, 2048], P('ep', 'tp'), may hold values from -16 to 16
- norm_gain: float32 [2048], P('tp'), may hold values from 0.1 to 1.9
- out_grad: bfloat16 [4096, 2048], P('ep', 'tp'), may hold values from -16 to 16
Outputs:
- token_grad: bfloat16 [4096, 2048], P(('ep', 'tp'))
- gates_grad: bfloat16 [4096, 2], P(('ep', 'tp'))
- w_gate_grad: bfloat16 [32, 2048, 768], P(('ep', 'tp'))
- w_up_grad: bfloat16 [32, 2048, 768], P(('ep', 'tp'))
- w_down_grad: bfloat16 [32, 768, 2048], P(('ep', 'tp'))
Inputs may be any that keep to these rules, and one draw needn't show every extreme that they name: `routes`: the two experts of a row differ and lie in one group (expert e is in group e // 8). In the 128 rows of one device the tokens fall into the groups in shares 3/8, 3/8, 1/8, 1/8 of 128, which group takes which share varying. In the rows of one device no expert is named more than 16 times, and one expert is named exactly 16 times in the rows of every device.
All inputs are finite; a program needn't handle non-finite values.
Results may differ from a plain program's by a relative error of at most 0.0071.
Values may be sent and summed in bfloat16 or wider, within the bound.
A program may use at most 128 MiB of HBM per device.

v0:
```python
import functools

import jax
import jax.numpy as jnp
from jax import lax
from jax.experimental import pallas as pl
from jax.experimental.pallas import tpu as pltpu
from jax.sharding import Mesh
from jax.sharding import PartitionSpec as P

epsilon = 1e-06
groups = 4
MESH = pl.DeviceIdType.MESH
AXES = ("z", "x", "tp")


def contract(left, right, left_dim, right_dim):
    return lax.dot_general(
        left, right, (((left_dim,), (right_dim,)), ((), ())), preferred_element_type=jnp.float32
    )


def earlier_equal(ids):
    count = ids.shape[-1]
    place = jnp.arange(count, dtype=jnp.int32)
    same = (ids[..., :, None] == ids[..., None, :]) & (place[:, None] > place[None, :])
    return jnp.sum(same.astype(jnp.int32), axis=-1)


def places(plane_size):
    z, x, t = (lax.axis_index(name) for name in AXES)
    z_count, t_count = lax.axis_size("z"), lax.axis_size("tp")
    own = x * t_count + t

    def z_peer(d):
        return (lax.rem(z + d, z_count), x, t)

    def plane_peer(k):
        q = lax.rem(own + k, plane_size)
        return q, (z, q // t_count, lax.rem(q, t_count))

    return z, own, z_count, z_peer, plane_peer


def enter(z_count, plane_size, z_peer, plane_peer):
    barrier = pltpu.get_barrier_semaphore()
    for d in range(1, z_count):
        pl.semaphore_signal(barrier, inc=1, device_id=z_peer(d), device_id_type=MESH)

    def greet(k, carry):
        pl.semaphore_signal(barrier, inc=1, device_id=plane_peer(k)[1], device_id_type=MESH)
        return carry

    lax.fori_loop(1, plane_size, greet, 0)
    pl.semaphore_wait(barrier, z_count - 1 + plane_size - 1)


def columns_dot(left, read, write, features):
    chunk = min(512, features)

    def one(c, carry):
        cols = pl.ds(pl.multiple_of(c * chunk, chunk), chunk)
        write(cols, jnp.dot(left, read(cols), preferred_element_type=jnp.float32))
        return carry

    lax.fori_loop(0, features // chunk, one, 0)


def dispatch_kernel(
    plane_size, slots, tok_ref, cot_ref, sel_ref, tok_out, cot_out,
    zbuf, sbuf, zs_sem, zr_sem, ps_sem, pr_sem, loc_sem,
):
    z, own, z_count, z_peer, plane_peer = places(plane_size)
    features = tok_ref.shape[-1]
    sends, outs = (tok_ref, cot_ref), (tok_out, cot_out)
    enter(z_count, plane_size, z_peer, plane_peer)

    def z_copy(a, d):
        return pltpu.make_async_remote_copy(
            src_ref=sends[a].at[lax.rem(z + d, z_count)],
            dst_ref=zbuf.at[a, d],
            send_sem=zs_sem.at[a, d],
            recv_sem=zr_sem.at[a, d],
            device_id=z_peer(d),
            device_id_type=MESH,
        )

    def rows_of(q):
        return pl.ds(pl.multiple_of(q * slots, slots), slots)

    def plane_copy(a, d, k):
        q, device = plane_peer(k)
        src = lax.rem(z + z_count - d, z_count)
        return pltpu.make_async_remote_copy(
            src_ref=sbuf.at[a, d, rows_of(q)],
            dst_ref=outs[a].at[src, rows_of(own)],
            send_sem=ps_sem.at[a, d, k],
            recv_sem=pr_sem.at[a, d, k],
            device_id=device,
            device_id_type=MESH,
        )

    def own_copy(a, d):
        src = lax.rem(z + z_count - d, z_count)
        return pltpu.make_async_copy(
            sbuf.at[a, d, rows_of(own)], outs[a].at[src, rows_of(own)], loc_sem.at[a, d]
        )

    for a in range(2):
        for d in range(1, z_count):
            z_copy(a, d).start()
    for a, d in [(0, 0), (1, 0)] + [(a, d) for a in range(2) for d in range(1, z_count)]:
        src = lax.rem(z + z_count - d, z_count)
        if d:
            z_copy(a, d).wait_recv()

        def read(cols):
            return zbuf[a, d, :, cols] if d else sends[a][z, :, cols]

        def write(cols, value):
            sbuf[a, d, :, cols] = value.astype(sbuf.dtype)

        columns_dot(sel_ref[src], read, write, features)
        lax.fori_loop(1, plane_size, lambda k, c: (plane_copy(a, d, k).start(), c)[1], 0)
        own_copy(a, d).start()
    for a in range(2):
        for d in range(z_count):
            if d:
                z_copy(a, d).wait_send()
            own_copy(a, d).wait()
            lax.fori_loop(1, plane_size, lambda k, c: (plane_copy(a, d, k).wait(), c)[1], 0)


def combine_kernel(
    plane_size, slots, back_ref, comb_ref, out_ref,
    rbuf, cbuf, zs_sem, zr_sem, ps_sem, pr_sem, loc_sem, own_sem,
):
    z, own, z_count, z_peer, plane_peer = places(plane_size)
    features = back_ref.shape[-1]
    enter(z_count, plane_size, z_peer, plane_peer)

    def rows_of(q):
        return pl.ds(pl.multiple_of(q * slots, slots), slots)

    def plane_copy(d, k):
        q, device = plane_peer(k)
        return pltpu.make_async_remote_copy(
            src_ref=back_ref.at[lax.rem(z + d, z_count), rows_of(q)],
            dst_ref=rbuf.at[d, rows_of(own)],
            send_sem=ps_sem.at[d, k],
            recv_sem=pr_sem.at[d, k],
            device_id=device,
            device_id_type=MESH,
        )

    def own_rows(d):
        return pltpu.make_async_copy(
            back_ref.at[lax.rem(z + d, z_count), rows_of(own)], rbuf.at[d, rows_of(own)], loc_sem.at[d]
        )

    def z_copy(d):
        return pltpu.make_async_remote_copy(
            src_ref=cbuf.at[d],
            dst_ref=out_ref.at[z],
            send_sem=zs_sem.at[d],
            recv_sem=zr_sem.at[d],
            device_id=z_peer(d),
            device_id_type=MESH,
        )

    keep = pltpu.make_async_copy(cbuf.at[0], out_ref.at[z], own_sem)
    order = list(range(1, z_count)) + [0]
    for d in order:
        own_rows(d).start()
        lax.fori_loop(1, plane_size, lambda k, c: (plane_copy(d, k).start(), c)[1], 0)
    for d in order:
        own_rows(d).wait()
        lax.fori_loop(1, plane_size, lambda k, c: (plane_copy(d, k).wait_recv(), c)[1], 0)

        def read(cols):
            return rbuf[d, :, cols]

        def write(cols, value):
            cbuf[d, :, cols] = value.astype(cbuf.dtype)

        columns_dot(comb_ref[lax.rem(z + d, z_count)], read, write, features)
        if d:
            z_copy(d).start()
        else:
            keep.start()
    for d in order:
        lax.fori_loop(1, plane_size, lambda k, c: (plane_copy(d, k).wait_send(), c)[1], 0)
        if d:
            z_copy(d).wait()
    keep.wait()


def dispatch(tok_send, cot_send, select, plane_size, slots):
    z_count, rows, features = tok_send.shape
    out = jax.ShapeDtypeStruct((z_count, plane_size * slots, features), tok_send.dtype)
    vmem, any_space = pl.BlockSpec(memory_space=pltpu.VMEM), pl.BlockSpec(memory_space=pl.ANY)
    dma = pltpu.SemaphoreType.DMA
    return pl.pallas_call(
        functools.partial(dispatch_kernel, plane_size, slots),
        out_shape=(out, out),
        in_specs=[vmem] * 3,
        out_specs=(any_space, any_space),
        scratch_shapes=[
            pltpu.VMEM((2, z_count, rows, features), tok_send.dtype),
            pltpu.VMEM((2,) + out.shape, tok_send.dtype),
            dma((2, z_count)),
            dma((2, z_count)),
            dma((2, z_count, plane_size)),
            dma((2, z_count, plane_size)),
            dma((2, z_count)),
        ],
        compiler_params=pltpu.CompilerParams(
            collective_id=0, has_side_effects=True, vmem_limit_bytes=48 * 1024 * 1024
        ),
        name="dispatch",
    )(tok_send, cot_send, select)


def combine(back, comb, plane_size, slots):
    z_count, _, features = back.shape
    rows = comb.shape[1]
    vmem, any_space = pl.BlockSpec(memory_space=pltpu.VMEM), pl.BlockSpec(memory_space=pl.ANY)
    dma = pltpu.SemaphoreType.DMA
    return pl.pallas_call(
        functools.partial(combine_kernel, plane_size, slots),
        out_shape=jax.ShapeDtypeStruct((z_count, rows, features), back.dtype),
        in_specs=[any_space, vmem],
        out_specs=any_space,
        scratch_shapes=[
            pltpu.VMEM(back.shape, back.dtype),
            pltpu.VMEM((z_count, rows, features), back.dtype),
            dma((z_count,)),
            dma((z_count,)),
            dma((z_count, plane_size)),
            dma((z_count, plane_size)),
            dma((z_count,)),
            dma(()),
        ],
        compiler_params=pltpu.CompilerParams(
            collective_id=1, has_side_effects=True, vmem_limit_bytes=48 * 1024 * 1024
        ),
        name="combine",
    )(back, comb)


def local(tokens, routes, gates, w_gate, w_up, w_down, moe_out, norm_gain, out_grad):
    z_count, x_count, t_count = (lax.axis_size(name) for name in AXES)
    plane_size = x_count * t_count
    devices = z_count * plane_size
    z, x, t = (lax.axis_index(name) for name in AXES)
    own = x * t_count + t
    me = z * plane_size + own
    tok_rows, features = tokens.shape
    top_count = routes.shape[1]
    capacity = groups * tok_rows // devices
    slots = -(-capacity // 16) * 16
    group_rows = 3 * tok_rows // 8
    route_count = tok_rows * top_count
    bf16 = jnp.bfloat16

    saved_out = moe_out.astype(jnp.float32)
    scaled = norm_gain[None, :] * out_grad.astype(jnp.float32)
    stats = jnp.stack([jnp.sum(saved_out * saved_out, axis=1), jnp.sum(saved_out * scaled, axis=1)])
    packed = jnp.concatenate(
        [stats.reshape(-1), routes.T.reshape(-1).astype(jnp.float32), gates.T.reshape(-1)]
    )
    gathered = lax.all_gather(packed, AXES, axis=0, tiled=False)
    stat_count = stats.size
    ep_stats = lax.dynamic_slice(gathered, (me - t, 0), (t_count, stat_count))
    square_sum, cross_sum = jnp.sum(ep_stats.reshape(t_count, 2, -1), axis=0)
    all_ids = gathered[:, stat_count : stat_count + route_count].astype(jnp.int32)
    all_gates = gathered[:, stat_count + route_count :].astype(bf16).astype(jnp.float32)

    inv_rms = lax.rsqrt(square_sum / features + epsilon)
    expert_cot = (
        inv_rms[:, None] * scaled - saved_out * (inv_rms**3 * cross_sum / features)[:, None]
    ).astype(bf16)
    cot_rows = lax.all_to_all(expert_cot, "tp", split_axis=0, concat_axis=1, tiled=True)

    own_ids = routes.T.reshape(-1)
    own_group = routes[:, 0] // plane_size
    z_slot = own_group * group_rows + earlier_equal(own_group)
    pack = (jnp.arange(groups * group_rows, dtype=jnp.int32)[:, None] == z_slot[None, :]).astype(bf16)
    tok_send = jnp.dot(pack, tokens, preferred_element_type=jnp.float32).astype(bf16)
    cot_send = jnp.dot(pack, cot_rows, preferred_element_type=jnp.float32).astype(bf16)

    ids = lax.dynamic_index_in_dim(
        all_ids.reshape(z_count, plane_size, route_count), own, axis=1, keepdims=False
    )
    slot_of = (ids - z * plane_size) * slots + earlier_equal(ids)
    slot_of = jnp.where(ids // plane_size == z, slot_of, -1)
    group_of = ids[:, :tok_rows] // plane_size
    row_of = jnp.where(group_of == z, earlier_equal(group_of), -1)
    row_of = jnp.tile(row_of, (1, top_count))
    at_slot = (
        slot_of[:, None, :] == jnp.arange(plane_size * slots, dtype=jnp.int32)[None, :, None]
    ).astype(bf16)
    at_row = (row_of[:, None, :] == jnp.arange(group_rows, dtype=jnp.int32)[None, :, None]).astype(bf16)
    select = jnp.einsum("zsf,zrf->zsr", at_slot, at_row, preferred_element_type=jnp.float32).astype(bf16)
    spread = jnp.einsum("zrf,zsf->zrs", at_row, at_slot, preferred_element_type=jnp.float32).astype(bf16)

    hit = all_ids == me
    hit_rank = jnp.cumsum(hit.astype(jnp.int32), axis=1) - 1
    chosen = hit[:, None, :] & (
        hit_rank[:, None, :] == jnp.arange(slots, dtype=jnp.int32)[None, :, None]
    )
    weight = jnp.sum(jnp.where(chosen, all_gates[:, None, :], 0.0), axis=2).reshape(-1)[:, None]

    token_in, cot_in = dispatch(
        tok_send.reshape(groups, group_rows, features),
        cot_send.reshape(groups, group_rows, features),
        select,
        plane_size,
        slots,
    )
    row_block = token_in.reshape(devices * slots, features)
    cot_in = cot_in.reshape(devices * slots, features)
    w_gate_one = w_gate[0]
    w_up_one = w_up[0]
    w_down_one = w_down[0]
    pre_gate = jnp.dot(row_block, w_gate_one, preferred_element_type=jnp.float32)
    pre_up = jnp.dot(row_block, w_up_one, preferred_element_type=jnp.float32)
    sigmoid_gate = jax.nn.sigmoid(pre_gate)
    activated = pre_gate * sigmoid_gate
    hidden = activated * pre_up
    hid_grad = contract(cot_in, w_down_one, 1, 1)
    gate_grad = jnp.sum(hidden * hid_grad, axis=1).astype(bf16)
    d_hidden = weight * hid_grad
    d_gate = (d_hidden * pre_up * sigmoid_gate * (1.0 + pre_gate * (1.0 - sigmoid_gate))).astype(bf16)
    d_up = (d_hidden * activated).astype(bf16)
    token_back = (contract(d_gate, w_gate_one, 1, 1) + contract(d_up, w_up_one, 1, 1)).astype(bf16)
    scaled_cot = (weight * cot_in.astype(jnp.float32)).astype(bf16)
    grad_gate = contract(row_block, d_gate, 0, 0).astype(bf16)
    grad_up = contract(row_block, d_up, 0, 0).astype(bf16)
    grad_down = contract(hidden.astype(bf16), scaled_cot, 0, 0).astype(bf16)

    back_gates = lax.all_to_all(
        gate_grad.reshape(devices, slots), AXES, split_axis=0, concat_axis=0, tiled=True
    )
    back = combine(
        token_back.reshape(z_count, plane_size * slots, features), spread, plane_size, slots
    )
    token_grad = contract(pack, back.reshape(groups * group_rows, features), 0, 0).astype(bf16)
    own_slots = own_ids * slots + earlier_equal(own_ids)
    picked = own_slots[:, None] == jnp.arange(devices * slots, dtype=jnp.int32)[None, :]
    gates_grad = jnp.sum(
        jnp.where(picked, back_gates.reshape(1, -1).astype(jnp.float32), 0.0), axis=1
    ).astype(bf16)
    gates_grad = gates_grad.reshape(top_count, tok_rows).T
    return (token_grad, gates_grad, grad_gate[None], grad_up[None], grad_down[None])


def solution(mesh):
    ep, tp = mesh.shape["ep"], mesh.shape["tp"]
    cut = Mesh(mesh.devices.reshape(groups, ep // groups, tp), AXES)
    rows, ep_axes = P(AXES, None), ("z", "x")
    cube = P(AXES, None, None)
    return jax.shard_map(
        local,
        mesh=cut,
        in_specs=(rows, rows, rows, cube, cube, cube, P(ep_axes, "tp"), P("tp"), P(ep_axes, "tp")),
        out_specs=(rows, rows, cube, cube, cube),
        check_vma=False,
    )
```

profile of v0, /device:TPU:0, one launch (start us, length us, event | category | flops | bytes accessed | tf_op | source)
XLA Modules:
  0.0 186.1 jit_solution(15363641608972613387)
XLA Ops:
  0.7 0.8 bitcast_convert_fusion
  1.5 1.6 fusion.17
  3.9 43.8 %all-gather.1 = f32[32,1,1536]{2,1,0:T(1,128)S(1)} all-gather(f32[1,1,1536]{2,1,0:T(1,128)S(1)} %reshape.220), channel_id=2, replica_groups=mesh['z'=4,'x'=2,'tp'=4] {'z','x','tp'}, dimensions={0}, use_global_device_ids=true | all-gather | bytes 202752 | tf_op jit(solution)/shard_map/all_gather | solution.py:272
  47.7 2.3 %fusion.20 = bf16[512,512]{1,0:T(8,128)(2,1)} fusion(bf16[512,512]{1,0:T(8,128)(2,1)} %param.15, bf16[512,512]{1,0:T(8,128)(2,1)} %param.17, f32[512]{0:T(512)S(1)} %get-tuple-element.17, f32[512]{0:T(512)S(1)} %get-tuple-element.16, f32[512]{0:T(512)} %param.16), kind=kLoop, calls=%fused_computation.35 | loop fusion | flops 1835008 | bytes 1579008 | tf_op jit(solution)/shard_map/convert_element_type | solution.py:282
  49.9 4.1 %all-to-all-start = ((bf16[4,128,512]{2,1,0:T(8,128)(2,1)}), bf16[4,128,512]{2,1,0:T(8,128)(2,1)}, u32[]{:S(2)}, u32[]{:S(2)}) async-start(bf16[4,128,512]{2,1,0:T(8,128)(2,1)} %bitcast.116), calls=%async_computation | async-start | bytes 1048576 | tf_op jit(solution)/shard_map/all_to_all | solution.py:283
  58.9 1.0 select_reduce_fusion.1
  60.1 0.8 convert_reduce_fusion.3
  61.0 2.3 %convolution_convert_fusion.4 = bf16[192,2048]{1,0:T(8,128)(2,1)} fusion(bf16[128,2048]{1,0:T(8,128)(2,1)} %param.9, s32[128]{0:T(128)S(1)} %multiply_add_fusion.1), kind=kOutput, calls=%fused_computation.19 | convolution fusion | flops 101081088 | bytes 1311232 | tf_op jit(solution)/shard_map/dot_general | solution.py:289
  63.3 2.0 %copy.35 = bf16[128,4,512]{0,2,1:T(8,128)(2,1)} copy(bf16[128,4,512]{2,0,1:T(8,128)(2,1)} %bitcast.10) | data formatting | bytes 1048576 | tf_op jit(solution)/shard_map/all_to_all | solution.py:283
  65.3 1.4 convolution_convert_fusion.3
  66.8 1.1 copy-done.1
  67.9 49.8 %dispatch.1 = (bf16[4,128,2048]{2,1,0:T(8,128)(2,1)S(1)}, bf16[4,128,2048]{2,1,0:T(8,128)(2,1)S(1)}) custom-call(bf16[4,48,2048]{2,1,0:T(8,128)(2,1)S(1)} %bitcast.105, bf16[4,48,2048]{2,1,0:T(8,128)(2,1)S(1)} %bitcast.106, bf16[4,128,48]{2,1,0:T(8,128)(2,1)S(1)} %copy.37.sel_ref), custom_call_target="tpu_custom_call" | custom-call | tf_op jit(solution)/shard_map/dispatch/pallas_call | solution.py:203
  117.7 3.7 %fusion.6 = f32[512,768]{1,0:T(8,128)S(1)} fusion(bf16[512,2048]{1,0:T(8,128)(2,1)S(1)} %bitcast.109, bf16[1,2048,768]{2,1,0:T(8,128)(2,1)} %param.13), kind=kOutput, calls=%fused_computation.11 | convolution fusion | flops 1610612736 | bytes 6815744 | tf_op jit(solution)/shard_map/dot_general | solution.py:327
  121.4 1.8 fusion.2
  123.3 2.5 %multiply_reduce_fusion = (bf16[512]{0:T(512)(128)(2,1)S(1)}, bf16[512,768]{1,0:T(8,128)(2,1)S(1)}, bf16[512,768]{1,0:T(8,128)(2,1)S(1)}) fusion(f32[512,768]{1,0:T(8,128)S(1)} %fusion.6, f32[512,768]{1,0:T(8,128)S(1)} %fusion.2, f32[512]{0:T(512)S(1)} %mul.119, bf16[512,2048]{1,0:T(8,128)(2,1)S(1)} %bitcast.113, bf16[1,768,2048]{2,1,0:T(8,128)(2,1)S(1)} %copy-done.4), kind=kOutput, calls=%fused_computation.22 | convolution fusion | flops 1617296896 | bytes 9964544 | tf_op jit(solution)/shard_map/dot_general | solution.py:18
  125.8 1.8 fusion
  127.6 3.5 %fusion.10 = bf16[1,2048,768]{2,1,0:T(8,128)(2,1)} fusion(bf16[512,2048]{1,0:T(8,128)(2,1)S(1)} %bitcast.111, bf16[512,768]{1,0:T(8,128)(2,1)S(1)} %get-tuple-element.14), kind=kOutput, calls=%fused_computation.15 | convolution fusion | flops 1612185600 | bytes 6029312 | tf_op jit(solution)/shard_map/dot_general | solution.py:18
  131.1 3.7 %fusion.12 = bf16[1,768,2048]{2,1,0:T(8,128)(2,1)} fusion(bf16[512,2048]{1,0:T(8,128)(2,1)S(1)} %bitcast.114, f32[512]{0:T(512)S(1)} %mul.119, f32[512,768]{1,0:T(8,128)S(1)} %fusion.6, f32[512,768]{1,0:T(8,128)S(1)} %fusion.2), kind=kOutput, calls=%fused_computation.17 | convolution fusion | flops 1617690624 | bytes 8390656 | tf_op jit(solution)/shard_map/dot_general | solution.py:18
  134.8 3.7 %fusion.11 = bf16[1,2048,768]{2,1,0:T(8,128)(2,1)} fusion(bf16[512,2048]{1,0:T(8,128)(2,1)S(1)} %bitcast.112, bf16[512,768]{1,0:T(8,128)(2,1)S(1)} %get-tuple-element.15), kind=kOutput, calls=%fused_computation.16 | convolution fusion | flops 1612185600 | bytes 6029312 | tf_op jit(solution)/shard_map/dot_general | solution.py:18
  138.6 3.2 %add_convert_fusion = bf16[512,2048]{1,0:T(8,128)(2,1)} fusion(f32[512,2048]{1,0:T(8,128)S(1)} %fusion, bf16[512,768]{1,0:T(8,128)(2,1)S(1)} %get-tuple-element.15, bf16[1,2048,768]{2,1,0:T(8,128)(2,1)S(1)} %copy-done.5), kind=kOutput, calls=%fused_computation.1 | convolution fusion | flops 1612709888 | bytes 10223616 | tf_op jit(solution)/shard_map/dot_general | solution.py:18
  142.4 7.5 %all-to-all-start.1 = ((bf16[32,1,16]{2,1,0:T(2,128)(2,1)}), bf16[32,1,16]{2,1,0:T(2,128)(2,1)S(1)}, u32[]{:S(2)}, u32[]{:S(2)}) async-start(bf16[32,1,16]{2,1,0:T(2,128)(2,1)} %convert_element_type.140), calls=%async_computation.1 | async-start | bytes 32768 | tf_op jit(solution)/shard_map/all_to_all | solution.py:342
  149.9 1.6 copy-done.2
  151.5 32.6 %combine.1 = bf16[4,48,2048]{2,1,0:T(8,128)(2,1)S(1)} custom-call(bf16[4,128,2048]{2,1,0:T(8,128)(2,1)S(1)} %bitcast.108, bf16[4,48,128]{2,1,0:T(8,128)(2,1)S(1)} %convolution_convert_fusion.6.comb_ref), custom_call_target="tpu_custom_call" | custom-call | tf_op jit(solution)/shard_map/combine/pallas_call | solution.py:229
  184.1 1.1 convolution_convert_fusion.5
  (52 shorter events, 7.4 us)
Async XLA Ops:
  0.6 120.8 %copy-start = (bf16[1,2048,768]{2,1,0:T(8,128)(2,1)S(1)}, bf16[1,2048,768]{2,1,0:T(8,128)(2,1)}, u32[]{:S(2)}) copy-start(bf16[1,2048,768]{2,1,0:T(8,128)(2,1)} %param.12) | copy-start | bytes 9437188
  0.6 53.4 %copy-start.3 = (s32[128,2]{0,1:T(2,128)S(1)}, s32[128,2]{0,1:T(2,128)}, u32[]{:S(2)}) copy-start(s32[128,2]{0,1:T(2,128)} %param.10) | copy-start | bytes 3076
  49.9 13.3 %all-to-all-start = ((bf16[4,128,512]{2,1,0:T(8,128)(2,1)}), bf16[4,128,512]{2,1,0:T(8,128)(2,1)}, u32[]{:S(2)}, u32[]{:S(2)}) async-start(bf16[4,128,512]{2,1,0:T(8,128)(2,1)} %bitcast.116), calls=%async_computation | async-start | bytes 1048576 | tf_op jit(solution)/shard_map/all_to_all | solution.py:283
  66.8 1.1 copy-start.1
  121.4 1.9 %copy-start.4 = (bf16[1,768,2048]{2,1,0:T(8,128)(2,1)S(1)}, bf16[1,768,2048]{2,1,0:T(8,128)(2,1)}, u32[]{:S(2)}) copy-start(bf16[1,768,2048]{2,1,0:T(8,128)(2,1)} %param.14) | copy-start | bytes 9437188
  134.8 3.7 %copy-start.5 = (bf16[1,2048,768]{2,1,0:T(8,128)(2,1)S(1)}, bf16[1,2048,768]{2,1,0:T(8,128)(2,1)}, u32[]{:S(2)}) copy-start(bf16[1,2048,768]{2,1,0:T(8,128)(2,1)} %param.13) | copy-start | bytes 9437188
  142.4 42.8 %all-to-all-start.1 = ((bf16[32,1,16]{2,1,0:T(2,128)(2,1)}), bf16[32,1,16]{2,1,0:T(2,128)(2,1)S(1)}, u32[]{:S(2)}, u32[]{:S(2)}) async-start(bf16[32,1,16]{2,1,0:T(2,128)(2,1)} %convert_element_type.140), calls=%async_computation.1 | async-start | bytes 32768 | tf_op jit(solution)/shard_map/all_to_all | solution.py:342
  149.9 1.6 copy-start.2
where the time goes:
time: 187 us; the launch traced here: 186 us
  Pallas kernels  82.4 us (44%)
  blocking collectives  43.8 us (23%)
  matrix products  29.2 us (16%)
  starting transfers between devices  11.6 us (6%)
  other arithmetic  11.4 us (6%)
  local copies, waits for them, and re-layouts  6.82 us (4%)
    pallas_call x1, Pallas kernels, dispatch(): pl.pallas_call(functools.partial(dispatch_kernel, plane_size, slots), out...  49.8 us
    all_gather x1, blocking collectives, local(): gathered = lax.all_gather(packed, AXES, axis=0, tiled=False)  43.8 us
    pallas_call x1, Pallas kernels, combine(): pl.pallas_call(functools.partial(combine_kernel, plane_size, slots), out_...  32.6 us
    dot_general x7, matrix products, contract(): lax.dot_general(left, right, (((left_dim,), (right_dim,)), ((), ())), pre...  19.6 us
    all_to_all x1, starting transfers between devices, local(): lax.all_to_all(gate_grad.reshape(devices, slots), AXES, split_axis=0, con...  7.47 us
    all_to_all x1, starting transfers between devices, local(): lax.all_to_all(expert_cot, 'tp', split_axis=0, concat_axis=1, tiled=True)  4.13 us
  transfers between devices with their start and end apart: 2, of which 0 were waited for; matrix products, arithmetic and copies ran while one was open for 5% of the time, Pallas kernels for 17%

commit v1 on v0

v1 whole, which is shorter than its diff:
```python
import functools

import jax
import jax.numpy as jnp
from jax import lax
from jax.experimental import pallas as pl
from jax.experimental.pallas import tpu as pltpu
from jax.sharding import Mesh
from jax.sharding import PartitionSpec as P

epsilon = 1e-06
groups = 4
MESH = pl.DeviceIdType.MESH
AXES = ("z", "x", "tp")
META_ROWS = 8
LANES = 128


def contract(left, right, left_dim, right_dim, **kw):
    return lax.dot_general(
        left, right, (((left_dim,), (right_dim,)), ((), ())), preferred_element_type=jnp.float32, **kw
    )


def earlier_equal(ids):
    count = ids.shape[-1]
    place = jnp.arange(count, dtype=jnp.int32)
    same = (ids[..., :, None] == ids[..., None, :]) & (place[:, None] > place[None, :])
    return jnp.sum(same.astype(jnp.int32), axis=-1)


class Place:
    def __init__(self, plane_size):
        self.z, self.x, self.t = (lax.axis_index(name) for name in AXES)
        self.zc, self.tc = lax.axis_size("z"), lax.axis_size("tp")
        self.plane = plane_size
        self.own = self.x * self.tc + self.t

    def at(self, d, k=0):
        return (lax.rem(self.z + d, self.zc), self.x, lax.rem(self.t + k, self.tc))

    def back(self, d):
        return (lax.rem(self.z + self.zc - d, self.zc), self.x, self.t)

    def peer(self, k):
        q = lax.rem(self.own + k, self.plane)
        return q, (self.z, q // self.tc, lax.rem(q, self.tc))


def enter(place, wide):
    barrier = pltpu.get_barrier_semaphore()

    def greet(device):
        pl.semaphore_signal(barrier, inc=1, device_id=device, device_id_type=MESH)

    lax.fori_loop(1, place.plane, lambda k, c: (greet(place.peer(k)[1]), c)[1], 0)
    across = place.tc if wide else 1
    for d in range(1, place.zc):
        lax.fori_loop(0, across, lambda k, c: (greet(place.at(d, k)), c)[1], 0)
    pl.semaphore_wait(barrier, place.plane - 1 + (place.zc - 1) * across)


def each(first, last, act):
    lax.fori_loop(first, last, lambda k, c: (act(k), c)[1], 0)


def columns(features, act):
    chunk = min(512, features)
    each(0, features // chunk, lambda c: act(pl.ds(pl.multiple_of(c * chunk, chunk), chunk)))


def iota(shape, dim):
    return lax.broadcasted_iota(jnp.int32, shape, dim)


def chosen(meta, row, slots, width):
    ids = meta[row : row + 1, :width].astype(jnp.int32)
    return iota((slots, width), 0) == ids


def picker(meta, slots, width):
    return (chosen(meta, 0, slots, width) | chosen(meta, 1, slots, width)).astype(
        jnp.float32
    ).astype(jnp.bfloat16)


def dispatch_kernel(
    plane_size, slots, tok_ref, meta_ref, saved_ref, grad_ref, gain_ref,
    tok_out, cot_out, w_out, meta_out,
    mbuf, stat, stbuf, cotz, ztok, zcot, stok, scot, wsend, wrecv,
    ms_sem, mr_sem, ss_sem, sr_sem, zs_sem, zr_sem, ps_sem, pr_sem, loc_sem, ws_sem, wr_sem,
):
    place = Place(plane_size)
    z, x, t, zc, tc = place.z, place.x, place.t, place.zc, place.tc
    own, peer = place.own, place.peer
    features = tok_ref.shape[-1]
    group_rows = tok_ref.shape[1]
    part = saved_ref.shape[-1]
    block = saved_ref.shape[0] // tc
    all_slots = plane_size * slots
    bf16 = jnp.bfloat16
    enter(place, True)

    def rows_of(q):
        return pl.ds(pl.multiple_of(q * slots, slots), slots)

    def remote(src, dst, send, recv, device):
        return pltpu.make_async_remote_copy(
            src_ref=src, dst_ref=dst, send_sem=send, recv_sem=recv, device_id=device, device_id_type=MESH
        )

    def meta_copy(d, k):
        return remote(
            meta_ref.at[lax.rem(z + d, zc)], mbuf.at[d, t], ms_sem.at[d, k], mr_sem.at[d, k], place.at(d, k)
        )

    def stat_copy(k):
        return remote(stat, stbuf.at[k], ss_sem.at[k], sr_sem.at[k], place.at(0, k))

    def z_copy(a, d):
        src, dst = ((tok_ref, ztok), (cotz, zcot))[a]
        return remote(
            src.at[lax.rem(z + d, zc)], dst.at[d], zs_sem.at[a, d], zr_sem.at[a, d], place.at(d)
        )

    def plane_parts(a, d, q):
        if a == 0:
            return stok.at[d, rows_of(q)], tok_out.at[d, rows_of(own)]
        cols = pl.ds(pl.multiple_of(t * part, part), part)
        return scot.at[d, :, rows_of(q)], cot_out.at[d, x, :, :, cols]

    def plane_copy(a, d, k):
        q, device = peer(k)
        src, dst = plane_parts(a, d, q)
        return remote(src, dst, ps_sem.at[a, d, k], pr_sem.at[a, d, k], device)

    def own_copy(a, d):
        src, dst = plane_parts(a, d, own)
        return pltpu.make_async_copy(src, dst, loc_sem.at[a, d])

    def w_copy(k):
        q, device = peer(k)
        return remote(wsend.at[rows_of(q)], wrecv.at[rows_of(own)], ws_sem.at[k], wr_sem.at[k], device)

    def spread_out(a, d):
        each(1, plane_size, lambda k: plane_copy(a, d, k).start())
        own_copy(a, d).start()

    def send_tok(d):
        sel = picker(mbuf[d, t], all_slots, group_rows)

        def one(cols):
            rows = ztok[d, :, cols] if d else tok_ref[z, :, cols]
            stok[d, :, cols] = jnp.dot(sel, rows, preferred_element_type=jnp.float32).astype(bf16)

        columns(features, one)
        spread_out(0, d)

    def send_cot(d):
        for b in range(tc):
            sel = picker(mbuf[d, b], all_slots, group_rows)
            rows = slice(b * group_rows, (b + 1) * group_rows)
            value = zcot[d, rows, :] if d else cotz[z, rows, :]
            scot[d, b] = jnp.dot(sel, value, preferred_element_type=jnp.float32).astype(bf16)
        spread_out(1, d)

    mbuf[0, t] = meta_ref[z]
    for d in range(zc):
        each(0 if d else 1, tc, lambda k: meta_copy(d, k).start())
    for d in range(1, zc):
        z_copy(0, d).start()

    eye = iota((block, block), 0) == iota((block, block), 1)
    gain = gain_ref[...]
    for b in range(tc):
        rows = slice(b * block, (b + 1) * block)
        saved = saved_ref[rows, :].astype(jnp.float32)
        scaled = gain * grad_ref[rows, :].astype(jnp.float32)
        for i, value in enumerate((saved * saved, saved * scaled)):
            total = jnp.sum(value, axis=1, keepdims=True)
            row = i * tc + b
            stat[row : row + 1, :] = jnp.sum(jnp.where(eye, total, 0.0), axis=0, keepdims=True)
    each(1, tc, lambda k: stat_copy(k).start())

    send_tok(0)

    each(1, tc, lambda k: stat_copy(k).wait_recv())
    each(1, tc, lambda k: meta_copy(0, k).wait_recv())
    totals = stat[...]
    for k in range(1, tc):
        totals = totals + stbuf[k]
    inv = lax.rsqrt(totals[:tc] / features + epsilon)
    coef = inv * inv * inv * totals[tc:] / features
    for b in range(tc):
        rows = slice(b * block, (b + 1) * block)
        saved = saved_ref[rows, :].astype(jnp.float32)
        scaled = gain * grad_ref[rows, :].astype(jnp.float32)
        inv_col = jnp.sum(jnp.where(eye, inv[b : b + 1], 0.0), axis=1, keepdims=True)
        coef_col = jnp.sum(jnp.where(eye, coef[b : b + 1], 0.0), axis=1, keepdims=True)
        cot = (inv_col * scaled - saved * coef_col).astype(bf16)
        pack = chosen(mbuf[0, b], 4, zc * group_rows, block).astype(jnp.float32).astype(bf16)
        packed = jnp.dot(pack, cot, preferred_element_type=jnp.float32).astype(bf16)
        for g in range(zc):
            cotz[g, b * group_rows : (b + 1) * group_rows, :] = packed[g * group_rows : (g + 1) * group_rows]
    for d in range(1, zc):
        z_copy(1, d).start()
    send_cot(0)

    for d in range(1, zc):
        each(0, tc, lambda k: meta_copy(d, k).wait_recv())
    weights = jnp.zeros((all_slots, LANES), jnp.float32)
    for d in range(zc):
        meta = mbuf[d, t]
        meta_out[d] = meta
        total = jnp.zeros((all_slots, 1), jnp.float32)
        for i in range(2):
            hit = chosen(meta, i, all_slots, group_rows)
            total = total + jnp.sum(
                jnp.where(hit, meta[2 + i : 3 + i, :group_rows], 0.0), axis=1, keepdims=True
            )
        weights = jnp.where(iota((all_slots, LANES), 1) == d, total, weights)
    wsend[...] = weights.astype(bf16)
    each(1, plane_size, lambda k: w_copy(k).start())
    wrecv[rows_of(own)] = wsend[rows_of(own)]

    for d in range(1, zc):
        z_copy(0, d).wait_recv()
        send_tok(d)
    for d in range(1, zc):
        z_copy(1, d).wait_recv()
        send_cot(d)

    each(1, plane_size, lambda k: w_copy(k).wait_recv())
    w_out[...] = wrecv[...]
    for a in range(2):
        for d in range(zc):
            own_copy(a, d).wait()
            each(1, plane_size, lambda k: plane_copy(a, d, k).wait(), )
            if d:
                z_copy(a, d).wait_send()
    for d in range(zc):
        each(0 if d else 1, tc, lambda k: meta_copy(d, k).wait_send())
    each(1, tc, lambda k: stat_copy(k).wait_send())
    each(1, plane_size, lambda k: w_copy(k).wait_send())


def combine_kernel(
    plane_size, slots, back_ref, gg_ref, meta_ref, out_ref, gout_ref,
    rbuf, cbuf, ggbuf, gbuf, gland, zs_sem, zr_sem, ps_sem, pr_sem, loc_sem, own_sem,
    gs_sem, gr_sem, gzs_sem, gzr_sem,
):
    place = Place(plane_size)
    z, zc, own, peer = place.z, place.zc, place.own, place.peer
    features = back_ref.shape[-1]
    group_rows = out_ref.shape[1]
    all_slots = plane_size * slots
    enter(place, False)

    def rows_of(q):
        return pl.ds(pl.multiple_of(q * slots, slots), slots)

    def remote(src, dst, send, recv, device):
        return pltpu.make_async_remote_copy(
            src_ref=src, dst_ref=dst, send_sem=send, recv_sem=recv, device_id=device, device_id_type=MESH
        )

    def plane_copy(d, k):
        q, device = peer(k)
        return remote(
            back_ref.at[d, rows_of(q)], rbuf.at[d, rows_of(own)], ps_sem.at[d, k], pr_sem.at[d, k], device
        )

    def own_rows(d):
        return pltpu.make_async_copy(back_ref.at[d, rows_of(own)], rbuf.at[d, rows_of(own)], loc_sem.at[d])

    def gg_copy(k):
        q, device = peer(k)
        return remote(gg_ref.at[rows_of(q)], ggbuf.at[rows_of(own)], gs_sem.at[k], gr_sem.at[k], device)

    def z_copy(d):
        return remote(cbuf.at[d], out_ref.at[z], zs_sem.at[d], zr_sem.at[d], place.back(d))

    def gz_copy(d):
        return remote(gbuf.at[d], gland.at[z], gzs_sem.at[d], gzr_sem.at[d], place.back(d))

    keep = pltpu.make_async_copy(cbuf.at[0], out_ref.at[z], own_sem)
    order = list(range(1, zc)) + [0]
    each(1, plane_size, lambda k: gg_copy(k).start())
    ggbuf[rows_of(own)] = gg_ref[rows_of(own)]
    for d in order:
        own_rows(d).start()
        each(1, plane_size, lambda k: plane_copy(d, k).start())
    each(1, plane_size, lambda k: gg_copy(k).wait_recv())
    returned = ggbuf[...].astype(jnp.float32)
    for d in order:
        meta = meta_ref[d]
        column = jnp.sum(
            jnp.where(iota(returned.shape, 1) == d, returned, 0.0), axis=1, keepdims=True
        )
        for i in range(2):
            hit = chosen(meta, i, all_slots, LANES)
            gbuf[d, i : i + 1, :] = jnp.sum(jnp.where(hit, column, 0.0), axis=0, keepdims=True)
        if d:
            gz_copy(d).start()
        else:
            gland[z] = gbuf[0]
    for d in order:
        own_rows(d).wait()
        each(1, plane_size, lambda k: plane_copy(d, k).wait_recv())
        sel = picker(meta_ref[d], all_slots, group_rows)

        def one(cols):
            cbuf[d, :, cols] = contract(sel, rbuf[d, :, cols], 0, 0).astype(cbuf.dtype)

        columns(features, one)
        if d:
            z_copy(d).start()
        else:
            keep.start()
    for d in order:
        each(1, plane_size, lambda k: plane_copy(d, k).wait_send())
        if d:
            gz_copy(d).wait()
            z_copy(d).wait()
    keep.wait()
    gout_ref[...] = gland[...]
    each(1, plane_size, lambda k: gg_copy(k).wait_send())


def vmem():
    return pl.BlockSpec(memory_space=pltpu.VMEM)


def anywhere():
    return pl.BlockSpec(memory_space=pl.ANY)


def dispatch(tok_send, meta, saved, grad, gain, plane_size, slots, tc):
    zc, group_rows, features = tok_send.shape
    part = saved.shape[1]
    rows = plane_size * slots
    bf16 = tok_send.dtype
    dma, struct, space = pltpu.SemaphoreType.DMA, jax.ShapeDtypeStruct, pltpu.VMEM
    f32 = jnp.float32
    return pl.pallas_call(
        functools.partial(dispatch_kernel, plane_size, slots),
        out_shape=(
            struct((zc, rows, features), bf16),
            struct((zc, plane_size // tc, tc, slots, features), bf16),
            struct((rows, LANES), bf16),
            struct(meta.shape, f32),
        ),
        in_specs=[vmem()] * 5,
        out_specs=(anywhere(), anywhere(), vmem(), vmem()),
        scratch_shapes=[
            space((zc, tc, META_ROWS, LANES), f32),
            space((2 * tc, LANES), f32),
            space((tc, 2 * tc, LANES), f32),
            space((zc, tc * group_rows, part), bf16),
            space((zc, group_rows, features), bf16),
            space((zc, tc * group_rows, part), bf16),
            space((zc, rows, features), bf16),
            space((zc, tc, rows, part), bf16),
            space((rows, LANES), bf16),
            space((rows, LANES), bf16),
            dma((zc, tc)),
            dma((zc, tc)),
            dma((tc,)),
            dma((tc,)),
            dma((2, zc)),
            dma((2, zc)),
            dma((2, zc, plane_size)),
            dma((2, zc, plane_size)),
            dma((2, zc)),
            dma((plane_size,)),
            dma((plane_size,)),
        ],
        compiler_params=pltpu.CompilerParams(
            collective_id=0, has_side_effects=True, vmem_limit_bytes=48 * 1024 * 1024
        ),
        name="dispatch",
    )(tok_send, meta, saved, grad, gain)


def combine(back, gg, meta, group_rows, plane_size, slots):
    zc, rows, features = back.shape
    dma, struct, space = pltpu.SemaphoreType.DMA, jax.ShapeDtypeStruct, pltpu.VMEM
    return pl.pallas_call(
        functools.partial(combine_kernel, plane_size, slots),
        out_shape=(struct((zc, group_rows, features), back.dtype), struct(meta.shape, meta.dtype)),
        in_specs=[anywhere(), vmem(), vmem()],
        out_specs=(anywhere(), vmem()),
        scratch_shapes=[
            space(back.shape, back.dtype),
            space((zc, group_rows, features), back.dtype),
            space(gg.shape, gg.dtype),
            space(meta.shape, meta.dtype),
            space(meta.shape, meta.dtype),
            dma((zc,)),
            dma((zc,)),
            dma((zc, plane_size)),
            dma((zc, plane_size)),
            dma((zc,)),
            dma(()),
            dma((plane_size,)),
            dma((plane_size,)),
            dma((zc,)),
            dma((zc,)),
        ],
        compiler_params=pltpu.CompilerParams(
            collective_id=1, has_side_effects=True, vmem_limit_bytes=48 * 1024 * 1024
        ),
        name="combine",
    )(back, gg, meta)


def local(tokens, routes, gates, w_gate, w_up, w_down, moe_out, norm_gain, out_grad):
    z_count, x_count, t_count = (lax.axis_size(name) for name in AXES)
    plane_size = x_count * t_count
    devices = z_count * plane_size
    tok_rows, features = tokens.shape
    top_count = routes.shape[1]
    capacity = groups * tok_rows // devices
    slots = -(-capacity // 16) * 16
    group_rows = 3 * tok_rows // 8
    rows = plane_size * slots
    bf16, f32 = jnp.bfloat16, jnp.float32

    own_ids = routes.T.reshape(-1)
    own_group = routes[:, 0] // plane_size
    z_slot = own_group * group_rows + earlier_equal(own_group)
    hit = jnp.arange(groups * group_rows, dtype=jnp.int32)[:, None] == z_slot[None, :]
    tok_send = jnp.dot(hit.astype(bf16), tokens, preferred_element_type=f32).astype(bf16)
    slot_of = (own_ids % plane_size) * slots + earlier_equal(own_ids)
    values = jnp.concatenate(
        [
            slot_of.reshape(top_count, tok_rows).astype(f32) + 1.0,
            gates.T.astype(bf16).astype(f32),
        ]
    )
    packed = contract(values, hit.astype(f32), 1, 1, precision=lax.Precision.HIGHEST)
    packed = packed - jnp.array([1.0, 1.0, 0.0, 0.0], f32)[:, None]
    packed = packed.reshape(2 * top_count, groups, group_rows).transpose(1, 0, 2)
    packed = jnp.pad(
        packed,
        ((0, 0), (0, 0), (0, LANES - group_rows)),
        constant_values=-1.0,
    )
    extra = jnp.broadcast_to(z_slot.astype(f32)[None, None, :], (groups, META_ROWS - 4, tok_rows))
    meta = jnp.concatenate([packed, extra], axis=1)

    token_in, cot_in, gate_in, meta_in = dispatch(
        tok_send.reshape(groups, group_rows, features),
        meta,
        moe_out,
        out_grad,
        norm_gain[None, :],
        plane_size,
        slots,
        t_count,
    )
    weight = gate_in[:, :z_count].astype(f32).T.reshape(-1)[:, None]
    row_block = token_in.reshape(devices * slots, features)
    cot_in = cot_in.reshape(devices * slots, features)
    w_gate_one = w_gate[0]
    w_up_one = w_up[0]
    w_down_one = w_down[0]
    pre_gate = jnp.dot(row_block, w_gate_one, preferred_element_type=f32)
    pre_up = jnp.dot(row_block, w_up_one, preferred_element_type=f32)
    sigmoid_gate = jax.nn.sigmoid(pre_gate)
    activated = pre_gate * sigmoid_gate
    hidden = activated * pre_up
    hid_grad = contract(cot_in, w_down_one, 1, 1)
    gate_grad = jnp.sum(hidden * hid_grad, axis=1).astype(bf16)
    d_hidden = weight * hid_grad
    d_gate = (d_hidden * pre_up * sigmoid_gate * (1.0 + pre_gate * (1.0 - sigmoid_gate))).astype(bf16)
    d_up = (d_hidden * activated).astype(bf16)
    token_back = (contract(d_gate, w_gate_one, 1, 1) + contract(d_up, w_up_one, 1, 1)).astype(bf16)
    scaled_cot = (weight * cot_in.astype(f32)).astype(bf16)
    grad_gate = contract(row_block, d_gate, 0, 0).astype(bf16)
    grad_up = contract(row_block, d_up, 0, 0).astype(bf16)
    grad_down = contract(hidden.astype(bf16), scaled_cot, 0, 0).astype(bf16)

    gg = jnp.pad(gate_grad.reshape(z_count, rows).T, ((0, 0), (0, LANES - z_count)))
    back, gback = combine(
        token_back.reshape(z_count, rows, features), gg, meta_in, group_rows, plane_size, slots
    )
    token_grad = contract(hit.astype(bf16), back.reshape(groups * group_rows, features), 0, 0).astype(bf16)
    gvals = gback[:, :top_count, :group_rows].transpose(1, 0, 2).reshape(top_count, groups * group_rows)
    gates_grad = jnp.sum(jnp.where(hit.T[:, None, :], gvals[None], 0.0), axis=2).astype(bf16)
    return (token_grad, gates_grad, grad_gate[None], grad_up[None], grad_down[None])


def solution(mesh):
    ep, tp = mesh.shape["ep"], mesh.shape["tp"]
    cut = Mesh(mesh.devices.reshape(groups, ep // groups, tp), AXES)
    rows, ep_axes = P(AXES, None), ("z", "x")
    cube = P(AXES, None, None)
    return jax.shard_map(
        local,
        mesh=cut,
        in_specs=(rows, rows, rows, cube, cube, cube, P(ep_axes, "tp"), P("tp"), P(ep_axes, "tp")),
        out_specs=(rows, rows, cube, cube, cube),
        check_vma=False,
    )
```

time: 187 us -> 142 us (0.76)
  blocking collectives: 43.8 us -> 0 us
  starting transfers between devices: 11.6 us -> 0 us
  Pallas kernels: 82.4 us -> 91.3 us
  matrix products: 29.2 us -> 37.1 us
  other arithmetic: 11.4 us -> 5.5 us
    all_gather x1 -> x0, blocking collectives: 43.8 us -> none  [local(): gathered = lax.all_gather(packed, AXES, axis=0, tiled=False)]
    all_to_all x2 -> x0, starting transfers between devices: 11.6 us -> none  [the longest x1 7.47 us: local(): lax.all_to_all(gate_grad.reshape(devices, slots), AXES, split_axis=0, con...]
    pallas_call x1, Pallas kernels: 49.8 us -> 59.9 us  [dispatch(): pl.pallas_call(functools.partial(dispatch_kernel, plane_size, slots), out...]
    dot_general x7 -> x8, matrix products: 19.6 us -> 25.6 us  [contract(): lax.dot_general(left, right, (((left_dim,), (right_dim,)), ((), ())), pre...]
    unnamed x18 -> x32, local copies, waits for them, and re-layouts: 2.85 us -> 6.13 us
    reduce_sum x4 -> x1, other arithmetic: 3.33 us -> 0.64 us  [local(): jnp.sum(jnp.where(hit.T[:, None, :], gvals[None], 0.0), axis=2).astype(bf16)]
    convert_element_type x4 -> x2, other arithmetic: 3.76 us -> 1.38 us  [the longest x1 0.7 us: local(): z_slot.astype(f32)[None, None, :]]
    all_to_all x1 -> x0, local copies, waits for them, and re-layouts: 2.04 us -> none  [local(): lax.all_to_all(expert_cot, 'tp', split_axis=0, concat_axis=1, tiled=True)]
  transfers between devices with their start and end apart: 2 -> 0, of which waited for: 0 -> 0; matrix products, arithmetic and copies ran while one was open for 5% -> 0% of each run, Pallas kernels for 17% -> 0%
where the time goes in v1:
time: 142 us; the launch traced here: 141 us
  Pallas kernels  91.3 us (64%)
  matrix products  37.1 us (26%)
  local copies, waits for them, and re-layouts  6.59 us (5%)
  other arithmetic  5.5 us (4%)
    pallas_call x1, Pallas kernels, dispatch(): pl.pallas_call(functools.partial(dispatch_kernel, plane_size, slots), out...  59.9 us
    pallas_call x1, Pallas kernels, combine(): pl.pallas_call(functools.partial(combine_kernel, plane_size, slots), out_...  31.5 us
    dot_general x8, matrix products, contract(): lax.dot_general(left, right, (((left_dim,), (right_dim,)), ((), ())), pre...  25.6 us
    dot_general x1, matrix products, local(): pre_up = jnp.dot(row_block, w_up_one, preferred_element_type=f32)  6.34 us
    unnamed x32, local copies, waits for them, and re-layouts  6.13 us
    dot_general x1, matrix products, local(): pre_gate = jnp.dot(row_block, w_gate_one, preferred_element_type=f32)  2.94 us

profile of v1, /device:TPU:0, one launch (start us, length us, event | category | flops | bytes accessed | tf_op | source)
XLA Modules:
  0.0 141.3 jit_solution(13425428790932492993)
XLA Ops:
  0.6 0.8 and_select_fusion.2
  1.5 0.8 fusion.30
  2.5 0.7 fusion.33
  3.2 2.3 %convolution_convert_fusion.3 = bf16[192,2048]{1,0:T(8,128)(2,1)} fusion(bf16[128,2048]{1,0:T(8,128)(2,1)} %param.10, s32[128]{0:T(128)S(1)} %get-tuple-element.18), kind=kOutput, calls=%fused_computation.18 | convolution fusion | flops 101081088 | bytes 1311232 | tf_op jit(solution)/shard_map/dot_general | solution.py:433
  5.4 0.7 convert_bitcast_fusion.1
  6.1 0.9 convert_reduce_fusion
  7.1 0.7 convert_add_fusion
  7.8 0.8 convolution_add_fusion
  8.8 1.1 copy-done.1
  9.9 1.0 copy-done.3
  10.9 1.0 copy-done.4
  12.0 0.7 copy-done.5
  12.6 59.9 %dispatch.1 = (bf16[4,128,2048]{2,1,0:T(8,128)(2,1)S(1)}, bf16[4,2,4,16,2048]{4,3,2,1,0:T(8,128)(2,1)S(1)}, bf16[128,128]{1,0:T(8,128)(2,1)S(1)}, f32[4,8,128]{2,1,0:T(8,128)S(1)}) custom-call(bf16[4,48,2048]{2,1,0:T(8,128)(2,1)S(1)} %bitcast.76, f32[4,8,128]{2,1,0:T(8,128)S(1)} %select_maximum_fusion.meta_ref, bf16[512,512]{1,0:T(8,128)(2,1)S(1)} %copy-done.3, ...), custom_call_target="tpu_custom_call" | custom-call | tf_op jit(solution)/shard_map/dispatch/pallas_call | solution.py:345
  72.5 6.3 %fusion.6 = f32[512,768]{1,0:T(8,128)} fusion(bf16[512,2048]{1,0:T(8,128)(2,1)S(1)} %bitcast.82, bf16[1,2048,768]{2,1,0:T(8,128)(2,1)} %param.14), kind=kOutput, calls=%fused_computation.11 | convolution fusion | flops 1610612736 | bytes 6815744 | tf_op jit(solution)/shard_map/dot_general | solution.py:469
  78.9 2.9 %fusion.2 = f32[512,768]{1,0:T(8,128)} fusion(bf16[512,2048]{1,0:T(8,128)(2,1)S(1)} %bitcast.83, bf16[1,2048,768]{2,1,0:T(8,128)(2,1)S(1)} %copy-done), kind=kOutput, calls=%fused_computation.7 | convolution fusion | flops 1610612736 | bytes 6815744 | tf_op jit(solution)/shard_map/dot_general | solution.py:468
  81.9 6.0 %multiply_reduce_fusion = (bf16[512]{0:T(512)(128)(2,1)S(1)}, bf16[512,768]{1,0:T(8,128)(2,1)S(1)}, bf16[512,768]{1,0:T(8,128)(2,1)S(1)}) fusion(f32[512,768]{1,0:T(8,128)} %fusion.6, f32[512,768]{1,0:T(8,128)} %fusion.2, f32[512]{0:T(512)S(1)} %bitcast.89, bf16[512,2048]{1,0:T(8,128)(2,1)} %bitcast.80, bf16[1,768,2048]{2,1,0:T(8,128)(2,1)} %param.15), kind=kOutput, calls=%fused_computation.21 | convolution fusion | flops 1617296896 | bytes 9964544 | tf_op jit(solution)/shard_map/dot_general | solution.py:20
  87.9 1.8 %fusion = f32[512,2048]{1,0:T(8,128)S(1)} fusion(bf16[512,768]{1,0:T(8,128)(2,1)S(1)} %get-tuple-element.20, bf16[1,2048,768]{2,1,0:T(8,128)(2,1)S(1)} %copy-done), kind=kOutput, calls=%fused_computation.5 | convolution fusion | flops 1610612736 | bytes 8126464 | tf_op jit(solution)/shard_map/dot_general | solution.py:20
  90.4 3.1 %add_convert_fusion = bf16[512,2048]{1,0:T(8,128)(2,1)} fusion(f32[512,2048]{1,0:T(8,128)S(1)} %fusion, bf16[512,768]{1,0:T(8,128)(2,1)S(1)} %get-tuple-element.21, bf16[1,2048,768]{2,1,0:T(8,128)(2,1)S(1)} %copy-done.10), kind=kOutput, calls=%fused_computation.1 | convolution fusion | flops 1612709888 | bytes 10223616 | tf_op jit(solution)/shard_map/dot_general | solution.py:20
  93.7 1.6 %copy-done.2 = bf16[512,2048]{1,0:T(8,128)(2,1)S(1)} copy-done((bf16[512,2048]{1,0:T(8,128)(2,1)S(1)}, bf16[512,2048]{1,0:T(8,128)(2,1)}, u32[]{:S(2)}) %copy-start.2) | copy-done | bytes 2097176
  95.2 31.5 %combine.1 = (bf16[4,48,2048]{2,1,0:T(8,128)(2,1)S(1)}, f32[4,8,128]{2,1,0:T(8,128)S(1)}) custom-call(bf16[4,128,2048]{2,1,0:T(8,128)(2,1)S(1)} %bitcast.77, bf16[128,128]{1,0:T(8,128)(2,1)S(1)} %pad.9.gg_ref, f32[4,8,128]{2,1,0:T(8,128)S(1)} %get-tuple-element.14.meta_ref), custom_call_target="tpu_custom_call" | custom-call | tf_op jit(solution)/shard_map/combine/pallas_call | solution.py:388
  126.7 1.1 convolution_convert_fusion.4
  128.6 5.4 %fusion.10 = bf16[1,2048,768]{2,1,0:T(8,128)(2,1)} fusion(bf16[512,2048]{1,0:T(8,128)(2,1)} %bitcast.84, bf16[512,768]{1,0:T(8,128)(2,1)} %copy-done.13), kind=kOutput, calls=%fused_computation.15 | convolution fusion | flops 1612185600 | bytes 6029312 | tf_op jit(solution)/shard_map/dot_general | solution.py:20
  134.1 3.5 %fusion.11 = bf16[1,2048,768]{2,1,0:T(8,128)(2,1)} fusion(bf16[512,2048]{1,0:T(8,128)(2,1)S(1)} %bitcast.85, bf16[512,768]{1,0:T(8,128)(2,1)S(1)} %copy-done.12), kind=kOutput, calls=%fused_computation.16 | convolution fusion | flops 1612185600 | bytes 6029312 | tf_op jit(solution)/shard_map/dot_general | solution.py:20
  137.6 3.7 %fusion.12 = bf16[1,768,2048]{2,1,0:T(8,128)(2,1)} fusion(bf16[512,2048]{1,0:T(8,128)(2,1)S(1)} %bitcast.81, f32[512]{0:T(512)S(1)} %bitcast.90, f32[512,768]{1,0:T(8,128)S(1)} %copy-done.14, f32[512,768]{1,0:T(8,128)S(1)} %copy-done.15), kind=kOutput, calls=%fused_computation.17 | convolution fusion | flops 1617690624 | bytes 8390656 | tf_op jit(solution)/shard_map/dot_general | solution.py:20
  (41 shorter events, 2.0 us)
Async XLA Ops:
  0.6 78.3 %copy-start = (bf16[1,2048,768]{2,1,0:T(8,128)(2,1)S(1)}, bf16[1,2048,768]{2,1,0:T(8,128)(2,1)}, u32[]{:S(2)}) copy-start(bf16[1,2048,768]{2,1,0:T(8,128)(2,1)} %param.13) | copy-start | bytes 9437188
  8.7 1.1 copy-start.1
  9.9 1.0 copy-start.3
  10.9 1.0 copy-start.4
  12.0 0.7 copy-start.5
  72.5 6.4 %copy-start.6 = (bf16[4,2,4,16,2048]{4,3,2,1,0:T(8,128)(2,1)}, bf16[4,2,4,16,2048]{4,3,2,1,0:T(8,128)(2,1)S(1)}, u32[]{:S(2)}) copy-start(bf16[4,2,4,16,2048]{4,3,2,1,0:T(8,128)(2,1)S(1)} %get-tuple-element.12) | copy-start | bytes 6291460
  72.5 6.4 %copy-start.8 = (bf16[4,128,2048]{2,1,0:T(8,128)(2,1)}, bf16[4,128,2048]{2,1,0:T(8,128)(2,1)S(1)}, u32[]{:S(2)}) copy-start(bf16[4,128,2048]{2,1,0:T(8,128)(2,1)S(1)} %get-tuple-element.13) | copy-start | bytes 6291460
  87.9 1.9 %copy-start.13 = (bf16[512,768]{1,0:T(8,128)(2,1)}, bf16[512,768]{1,0:T(8,128)(2,1)S(1)}, u32[]{:S(2)}) copy-start(bf16[512,768]{1,0:T(8,128)(2,1)S(1)} %get-tuple-element.20) | copy-start | bytes 2359300
  87.9 1.9 %copy-start.11 = (bf16[512,768]{1,0:T(8,128)(2,1)}, bf16[512,768]{1,0:T(8,128)(2,1)S(1)}, u32[]{:S(2)}) copy-start(bf16[512,768]{1,0:T(8,128)(2,1)S(1)} %get-tuple-element.21) | copy-start | bytes 2359300
  87.9 2.5 %copy-start.10 = (bf16[1,2048,768]{2,1,0:T(8,128)(2,1)S(1)}, bf16[1,2048,768]{2,1,0:T(8,128)(2,1)}, u32[]{:S(2)}) copy-start(bf16[1,2048,768]{2,1,0:T(8,128)(2,1)} %param.14) | copy-start | bytes 9437188
  93.7 1.6 %copy-start.2 = (bf16[512,2048]{1,0:T(8,128)(2,1)S(1)}, bf16[512,2048]{1,0:T(8,128)(2,1)}, u32[]{:S(2)}) copy-start(bf16[512,2048]{1,0:T(8,128)(2,1)} %add_convert_fusion) | copy-start | bytes 6291460
  128.6 5.4 %copy-start.9 = (bf16[4,128,2048]{2,1,0:T(8,128)(2,1)S(1)}, bf16[4,128,2048]{2,1,0:T(8,128)(2,1)}, u32[]{:S(2)}) copy-start(bf16[4,128,2048]{2,1,0:T(8,128)(2,1)} %copy-done.8) | copy-start | bytes 6291460
  128.6 5.4 %copy-start.12 = (bf16[512,768]{1,0:T(8,128)(2,1)S(1)}, bf16[512,768]{1,0:T(8,128)(2,1)}, u32[]{:S(2)}) copy-start(bf16[512,768]{1,0:T(8,128)(2,1)} %copy-done.11) | copy-start | bytes 2359300
  134.1 3.6 %copy-start.7 = (bf16[4,2,4,16,2048]{4,3,2,1,0:T(8,128)(2,1)S(1)}, bf16[4,2,4,16,2048]{4,3,2,1,0:T(8,128)(2,1)}, u32[]{:S(2)}) copy-start(bf16[4,2,4,16,2048]{4,3,2,1,0:T(8,128)(2,1)} %copy-done.6) | copy-start | bytes 6291460
  134.1 3.6 %copy-start.14 = (f32[512,768]{1,0:T(8,128)S(1)}, f32[512,768]{1,0:T(8,128)}, u32[]{:S(2)}) copy-start(f32[512,768]{1,0:T(8,128)} %fusion.6) | copy-start | bytes 4718596
  134.1 3.6 %copy-start.15 = (f32[512,768]{1,0:T(8,128)S(1)}, f32[512,768]{1,0:T(8,128)}, u32[]{:S(2)}) copy-start(f32[512,768]{1,0:T(8,128)} %fusion.2) | copy-start | bytes 4718596

commit v2 on v1

--- a/solution.py
+++ b/solution.py
@@ -48,6 +48,11 @@
 
 
 def enter(place, wide):
+    wait = greet_all(place, wide)
+    wait()
+
+
+def greet_all(place, wide):
     barrier = pltpu.get_barrier_semaphore()
 
     def greet(device):
@@ -57,7 +62,7 @@
     across = place.tc if wide else 1
     for d in range(1, place.zc):
         lax.fori_loop(0, across, lambda k, c: (greet(place.at(d, k)), c)[1], 0)
-    pl.semaphore_wait(barrier, place.plane - 1 + (place.zc - 1) * across)
+    return lambda: pl.semaphore_wait(barrier, place.plane - 1 + (place.zc - 1) * across)
 
 
 def each(first, last, act):
@@ -414,7 +419,7 @@
     )(back, gg, meta)
 
 
-def local(tokens, routes, gates, w_gate, w_up, w_down, moe_out, norm_gain, out_grad):
+def apart(tokens, routes, gates, w_gate, w_up, w_down, moe_out, norm_gain, out_grad):
     z_count, x_count, t_count = (lax.axis_size(name) for name in AXES)
     plane_size = x_count * t_count
     devices = z_count * plane_size
@@ -491,6 +496,535 @@
     return (token_grad, gates_grad, grad_gate[None], grad_up[None], grad_down[None])
 
 
+def fused_kernel(
+    plane_size, slots, tok_hbm, route_hbm, gate_hbm, saved_hbm, grad_hbm, gain_hbm, wg_hbm, wu_hbm, wd_hbm,
+    tg_ref, gg_out, dwg_ref, dwu_ref, dwd_ref,
+    route_ref, gate_ref, gain_ref, tok, saved_ref, grad_ref, wg, wu, wd, meta, mbuf, stat, stbuf, tokz, cotz, ztok, zcot, stok, scot,
+    wsend, wrecv, tok_in, cot_in, hid, dg, du, back, rbuf, cbuf, land, ggsend, ggbuf, gbuf, gland,
+    in_sem, ms_sem, mr_sem, ss_sem, sr_sem, zs_sem, zr_sem, ps_sem, pr_sem, ws_sem, wr_sem,
+    rs_sem, rr_sem, os_sem, or_sem, gs_sem, gr_sem, gzs_sem, gzr_sem,
+):
+    place = Place(plane_size)
+    z, x, t, zc, tc = place.z, place.x, place.t, place.zc, place.tc
+    own, peer = place.own, place.peer
+    block, features = tok.shape
+    part = saved_ref.shape[-1]
+    group_rows = tokz.shape[1]
+    chunk = plane_size * slots
+    width = wg.shape[-1]
+    bf16, f32 = jnp.bfloat16, jnp.float32
+
+    loads = [
+        pltpu.make_async_copy(src, dst, in_sem.at[i])
+        for i, (src, dst) in enumerate(
+            (
+                (route_hbm, route_ref),
+                (gate_hbm, gate_ref),
+                (tok_hbm, tok),
+                (gain_hbm, gain_ref),
+                (saved_hbm, saved_ref),
+                (grad_hbm, grad_ref),
+                (wg_hbm.at[0], wg),
+                (wu_hbm.at[0], wu),
+                (wd_hbm.at[0], wd),
+            )
+        )
+    ]
+    for load in loads[:6]:
+        load.start()
+    everyone = greet_all(place, True)
+
+    def rows_of(q):
+        return pl.ds(pl.multiple_of(q * slots, slots), slots)
+
+    def chunk_rows(d, q):
+        return pl.ds(pl.multiple_of(d * chunk + q * slots, slots), slots)
+
+    def remote(src, dst, send, recv, device):
+        return pltpu.make_async_remote_copy(
+            src_ref=src, dst_ref=dst, send_sem=send, recv_sem=recv, device_id=device, device_id_type=MESH
+        )
+
+    def meta_copy(d, k):
+        return remote(
+            meta.at[lax.rem(z + d, zc)], mbuf.at[d, t], ms_sem.at[d, k], mr_sem.at[d, k], place.at(d, k)
+        )
+
+    def stat_copy(k):
+        return remote(stat, stbuf.at[k], ss_sem.at[k], sr_sem.at[k], place.at(0, k))
+
+    def z_copy(a, d):
+        src, dst = ((tokz, ztok), (cotz, zcot))[a]
+        return remote(
+            src.at[lax.rem(z + d, zc)], dst.at[d], zs_sem.at[a, d], zr_sem.at[a, d], place.at(d)
+        )
+
+    def plane_parts(a, d, q):
+        if a == 0:
+            return stok.at[d, rows_of(q)], tok_in.at[chunk_rows(d, own)]
+        cols = pl.ds(pl.multiple_of(t * part, part), part)
+        span = tc * slots
+        rows = pl.ds(pl.multiple_of(d * chunk + x * span, span), span)
+        return scot.at[d, q], cot_in.at[rows, cols]
+
+    def plane_copy(a, d, k):
+        q, device = peer(k)
+        src, dst = plane_parts(a, d, q)
+        return remote(src, dst, ps_sem.at[a, d, k], pr_sem.at[a, d, k], device)
+
+    def w_copy(k):
+        q, device = peer(k)
+        return remote(wsend.at[rows_of(q)], wrecv.at[rows_of(own)], ws_sem.at[k], wr_sem.at[k], device)
+
+    def return_copy(d, k):
+        q, device = peer(k)
+        return remote(
+            back.at[d, rows_of(q)], rbuf.at[d, rows_of(own)], rs_sem.at[d, k], rr_sem.at[d, k], device
+        )
+
+    def out_copy(d):
+        return remote(cbuf.at[d], land.at[z], os_sem.at[d], or_sem.at[d], place.back(d))
+
+    def gg_copy(k):
+        q, device = peer(k)
+        return remote(ggsend.at[rows_of(q)], ggbuf.at[rows_of(own)], gs_sem.at[k], gr_sem.at[k], device)
+
+    def gz_copy(d):
+        return remote(gbuf.at[d], gland.at[z], gzs_sem.at[d], gzr_sem.at[d], place.back(d))
+
+    def to_peers(copy):
+        each(1, plane_size, lambda k: copy(k).start())
+
+    def send_tok(d):
+        sel = picker(mbuf[d, t], chunk, group_rows)
+
+        def one(cols):
+            rows = ztok[d, :, cols] if d else tokz[z, :, cols]
+            stok[d, :, cols] = jnp.dot(sel, rows, preferred_element_type=f32).astype(bf16)
+
+        columns(features, one)
+        to_peers(lambda k: plane_copy(0, d, k))
+        tok_in[chunk_rows(d, own), :] = stok[d, rows_of(own), :]
+
+    def send_cot(d):
+        for b in range(tc):
+            sel = picker(mbuf[d, b], chunk, group_rows)
+            rows = slice(b * group_rows, (b + 1) * group_rows)
+            value = zcot[d, rows, :] if d else cotz[z, rows, :]
+            value = jnp.dot(sel, value, preferred_element_type=f32).astype(bf16)
+            for q in range(plane_size):
+                scot[d, q, b * slots : (b + 1) * slots, :] = value[q * slots : (q + 1) * slots]
+        to_peers(lambda k: plane_copy(1, d, k))
+        src, dst = plane_parts(1, d, own)
+        dst[...] = src[...]
+
+    eye = iota((block, block), 0) == iota((block, block), 1)
+    before = iota((block, block), 0) < iota((block, block), 1)
+
+    def column(row):
+        return jnp.sum(jnp.where(eye, row, 0.0), axis=1, keepdims=True)
+
+    def count(mask):
+        return jnp.sum(mask.astype(f32), axis=0, keepdims=True)
+
+    loads[0].wait()
+    loads[1].wait()
+    ids = route_ref[...].astype(f32)
+    ids = [ids[i : i + 1] for i in range(2)]
+    id_cols = [column(row) for row in ids]
+    group = sum((ids[0] >= float(g * plane_size)).astype(f32) for g in range(1, zc))
+    z_slot = group * group_rows + count((column(group) == group) & before)
+    ranks = [
+        count((id_cols[0] == ids[0]) & before),
+        count(id_cols[0] == ids[1]) + count((id_cols[1] == ids[1]) & before),
+    ]
+    values = [(ids[i] - group * plane_size) * slots + ranks[i] + 1.0 for i in range(2)]
+    values += [gate_ref[i : i + 1].astype(bf16).astype(f32) for i in range(2)]
+    value_cols = [column(row) for row in values]
+    slot_col = column(z_slot)
+    lane = iota((block, block), 1).astype(f32)
+    for g in range(zc):
+        hit = (slot_col == lane + float(g * group_rows)) & (lane < float(group_rows))
+        for i in range(4):
+            row = jnp.sum(jnp.where(hit, value_cols[i], 0.0), axis=0, keepdims=True)
+            meta[g, i : i + 1, :] = row - 1.0 if i < 2 else row
+        meta[g, 4:8, :] = jnp.broadcast_to(z_slot, (4, block))
+
+    def packer(row):
+        slot = iota((zc * group_rows, block), 0).astype(f32)
+        return (slot == row).astype(f32).astype(bf16)
+
+    own_pack = packer(z_slot)
+    loads[2].wait()
+
+    def pack_tokens(cols):
+        value = jnp.dot(own_pack, tok[:, cols], preferred_element_type=f32).astype(bf16)
+        for g in range(zc):
+            tokz[g, :, cols] = value[g * group_rows : (g + 1) * group_rows]
+
+    columns(features, pack_tokens)
+    everyone()
+
+    for d in range(zc):
+        each(0 if d else 1, tc, lambda k: meta_copy(d, k).start())
+    for d in range(1, zc):
+        z_copy(0, d).start()
+    mbuf[0, t] = meta[z]
+
+    for load in loads[6:]:
+        load.start()
+    for load in loads[3:6]:
+        load.wait()
+    gain = gain_ref[...]
+    for b in range(tc):
+        rows = slice(b * block, (b + 1) * block)
+        saved = saved_ref[rows, :].astype(f32)
+        scaled = gain * grad_ref[rows, :].astype(f32)
+        for i, value in enumerate((saved * saved, saved * scaled)):
+            total = jnp.sum(value, axis=1, keepdims=True)
+            row = i * tc + b
+            stat[row : row + 1, :] = jnp.sum(jnp.where(eye, total, 0.0), axis=0, keepdims=True)
+    each(1, tc, lambda k: stat_copy(k).start())
+
+    send_tok(0)
+
+    each(1, tc, lambda k: stat_copy(k).wait_recv())
+    each(1, tc, lambda k: meta_copy(0, k).wait_recv())
+    totals = stat[...]
+    for k in range(1, tc):
+        totals = totals + stbuf[k]
+    inv = lax.rsqrt(totals[:tc] / features + epsilon)
+    coef = inv * inv * inv * totals[tc:] / features
+    for b in range(tc):
+        rows = slice(b * block, (b + 1) * block)
+        saved = saved_ref[rows, :].astype(f32)
+        scaled = gain * grad_ref[rows, :].astype(f32)
+        cot = (column(inv[b : b + 1]) * scaled - saved * column(coef[b : b + 1])).astype(bf16)
+        packed = jnp.dot(packer(mbuf[0, b, 4:5, :]), cot, preferred_element_type=f32).astype(bf16)
+        for g in range(zc):
+            cotz[g, b * group_rows : (b + 1) * group_rows, :] = packed[g * group_rows : (g + 1) * group_rows]
+    for d in range(1, zc):
+        z_copy(1, d).start()
+    send_cot(0)
+
+    for d in range(1, zc):
+        each(0, tc, lambda k: meta_copy(d, k).wait_recv())
+    weights = jnp.zeros((chunk, LANES), f32)
+    for d in range(zc):
+        tile = mbuf[d, t]
+        total = jnp.zeros((chunk, 1), f32)
+        for i in range(2):
+            hit = chosen(tile, i, chunk, group_rows)
+            total = total + jnp.sum(
+                jnp.where(hit, tile[2 + i : 3 + i, :group_rows], 0.0), axis=1, keepdims=True
+            )
+        weights = jnp.where(iota((chunk, LANES), 1) == d, total, weights)
+    wsend[...] = weights.astype(bf16)
+    to_peers(w_copy)
+    wrecv[rows_of(own)] = wsend[rows_of(own)]
+
+    def weight_of(d):
+        tile = wrecv[...].astype(f32)
+        return jnp.sum(jnp.where(iota(tile.shape, 1) == d, tile, 0.0), axis=1, keepdims=True)
+
+    def compute(d):
+        rows = slice(d * chunk, (d + 1) * chunk)
+        for a in range(2):
+            each(1, plane_size, lambda k: plane_copy(a, d, k).wait_recv())
+        weight = weight_of(d)
+        step = 256
+
+        def forward(c, total):
+            cols = pl.ds(pl.multiple_of(c * step, step), step)
+            token = tok_in[rows, :]
+            pre_gate = jnp.dot(token, wg[:, cols], preferred_element_type=f32)
+            pre_up = jnp.dot(token, wu[:, cols], preferred_element_type=f32)
+            hid_grad = contract(cot_in[rows, :], wd[cols, :], 1, 1)
+            sigmoid = jax.nn.sigmoid(pre_gate)
+            activated = pre_gate * sigmoid
+            hidden = activated * pre_up
+            d_hidden = weight * hid_grad
+            hid[rows, cols] = hidden.astype(bf16)
+            dg[rows, cols] = (d_hidden * pre_up * sigmoid * (1.0 + pre_gate * (1.0 - sigmoid))).astype(bf16)
+            du[rows, cols] = (d_hidden * activated).astype(bf16)
+            return total + jnp.sum(hidden * hid_grad, axis=1, keepdims=True)
+
+        total = lax.fori_loop(0, width // step, forward, jnp.zeros((chunk, 1), f32))
+
+        def backward(cols):
+            value = contract(dg[rows, :], wg[cols, :], 1, 1) + contract(du[rows, :], wu[cols, :], 1, 1)
+            back[d, :, cols] = value.astype(bf16)
+            cot_in[rows, cols] = (weight * cot_in[rows, cols].astype(f32)).astype(bf16)
+
+        columns(features, backward)
+        return total
+
+    def give_back(d):
+        to_peers(lambda k: return_copy(d, k))
+        rbuf[d, rows_of(own)] = back[d, rows_of(own)]
+
+    def unite(d):
+        each(1, plane_size, lambda k: return_copy(d, k).wait_recv())
+        sel = picker(mbuf[d, t], chunk, group_rows)
+
+        def one(cols):
+            value = contract(sel, rbuf[d, :, cols], 0, 0).astype(bf16)
+            if d:
+                cbuf[d, :, cols] = value
+            else:
+                land[z, :, cols] = value
+
+        columns(features, one)
+        if d:
+            out_copy(d).start()
+
+    def weight_grad(out, left, right):
+        step = min(256, out.shape[0])
+
+        def one(c):
+            cols = pl.ds(pl.multiple_of(c * step, step), step)
+            out[cols, :] = contract(left[:, cols], right[...], 0, 0).astype(bf16)
+
+        each(0, out.shape[0] // step, one)
+
+    sums = [None] * zc
+    for d in range(1, zc):
+        z_copy(0, d).wait_recv()
+        send_tok(d)
+        if d == 1:
+            for load in loads[6:]:
+                load.wait()
+            each(1, plane_size, lambda k: w_copy(k).wait_recv())
+            sums[0] = compute(0)
+    for d in range(1, zc):
+        z_copy(1, d).wait_recv()
+        send_cot(d)
+    for d in range(1, zc):
+        sums[d] = compute(d)
+        if d < zc - 1:
+            give_back(d)
+    tile = jnp.zeros((chunk, LANES), f32)
+    for d in range(zc):
+        tile = jnp.where(iota((chunk, LANES), 1) == d, sums[d], tile)
+    ggsend[...] = tile.astype(bf16)
+    to_peers(gg_copy)
+    ggbuf[rows_of(own)] = ggsend[rows_of(own)]
+    give_back(zc - 1)
+    give_back(0)
+
+    grads = [(dwg_ref, tok_in, dg), (dwu_ref, tok_in, du), (dwd_ref, hid, cot_in)]
+    for d in range(1, zc):
+        unite(d)
+        if grads:
+            weight_grad(*grads.pop(0))
+    each(1, plane_size, lambda k: gg_copy(k).wait_recv())
+    returned = ggbuf[...].astype(f32)
+    for d in range(zc):
+        picked = jnp.sum(jnp.where(iota(returned.shape, 1) == d, returned, 0.0), axis=1, keepdims=True)
+        for i in range(2):
+            hit = chosen(mbuf[d, t], i, chunk, LANES)
+            gbuf[d, i : i + 1, :] = jnp.sum(jnp.where(hit, picked, 0.0), axis=0, keepdims=True)
+        if d:
+            gz_copy(d).start()
+    gland[z] = gbuf[0]
+    unite(0)
+
+    for d in range(1, zc):
+        gz_copy(d).wait_recv()
+        out_copy(d).wait_recv()
+
+    def unpack(cols):
+        total = jnp.zeros((block, cols.size), f32)
+        for g in range(zc):
+            total = total + contract(own_pack[g * group_rows : (g + 1) * group_rows], land[g, :, cols], 0, 0)
+        tg_ref[:, cols] = total.astype(bf16)
+
+    columns(features, unpack)
+    slot_col = column(mbuf[0, t, 4:5, :])
+    slot_row = mbuf[0, t, 4:5, :]
+    for i in range(2):
+        row = jnp.zeros((1, block), f32)
+        for g in range(zc):
+            source = column(gland[g, i : i + 1, :])
+            hit = iota((block, block), 0).astype(f32) + float(g * group_rows) == slot_row
+            hit = hit & (iota((block, block), 0) < group_rows)
+            row = row + jnp.sum(jnp.where(hit, source, 0.0), axis=0, keepdims=True)
+        gg_out[i : i + 1, :] = row
+
+    for d in range(zc):
+        each(0 if d else 1, tc, lambda k: meta_copy(d, k).wait_send())
+        for a in range(2):
+            each(1, plane_size, lambda k: plane_copy(a, d, k).wait_send())
+            if d:
+                z_copy(a, d).wait_send()
+        each(1, plane_size, lambda k: return_copy(d, k).wait_send())
+        if d:
+            out_copy(d).wait_send()
+            gz_copy(d).wait_send()
+    each(1, tc, lambda k: stat_copy(k).wait_send())
+    each(1, plane_size, lambda k: w_copy(k).wait_send())
+    each(1, plane_size, lambda k: gg_copy(k).wait_send())
+
+
+def fused_scratch(block, features, part, width, group_rows, zc, tc, plane_size, slots):
+    bf16, f32, space = jnp.bfloat16, jnp.float32, pltpu.VMEM
+    rows = plane_size * slots
+    tile = (META_ROWS, LANES)
+    return [
+        space((2, block), jnp.int32),
+        space((2, block), f32),
+        space((1, part), f32),
+        space((block, features), bf16),
+        space((tc * block, part), bf16),
+        space((tc * block, part), bf16),
+        space((features, width), bf16),
+        space((features, width), bf16),
+        space((width, features), bf16),
+        space((zc,) + tile, f32),
+        space((zc, tc) + tile, f32),
+        space((2 * tc, LANES), f32),
+        space((tc, 2 * tc, LANES), f32),
+        space((zc, group_rows, features), bf16),
+        space((zc, tc * group_rows, part), bf16),
+        space((zc, group_rows, features), bf16),
+        space((zc, tc * group_rows, part), bf16),
+        space((zc, rows, features), bf16),
+        space((zc, plane_size, tc * slots, part), bf16),
+        space((rows, LANES), bf16),
+        space((rows, LANES), bf16),
+        space((zc * rows, features), bf16),
+        space((zc * rows, features), bf16),
+        space((zc * rows, width), bf16),
+        space((zc * rows, width), bf16),
+        space((zc * rows, width), bf16),
+        space((zc, rows, features), bf16),
+        space((zc, rows, features), bf16),
+        space((zc, group_rows, features), bf16),
+        space((zc, group_rows, features), bf16),
+        space((rows, LANES), bf16),
+        space((rows, LANES), bf16),
+        space((zc,) + tile, f32),
+        space((zc,) + tile, f32),
+    ]
+
+
+def fused(tokens, routes, gates, saved, grad, gain, w_gate, w_up, w_down, scratch, limit, plane_size, slots, zc, tc):
+    dma, struct = pltpu.SemaphoreType.DMA, jax.ShapeDtypeStruct
+    bf16, f32 = jnp.bfloat16, jnp.float32
+    semaphores = [
+        dma((9,)),
+        dma((zc, tc)),
+        dma((zc, tc)),
+        dma((tc,)),
+        dma((tc,)),
+        dma((2, zc)),
+        dma((2, zc)),
+        dma((2, zc, plane_size)),
+        dma((2, zc, plane_size)),
+        dma((plane_size,)),
+        dma((plane_size,)),
+        dma((zc, plane_size)),
+        dma((zc, plane_size)),
+        dma((zc,)),
+        dma((zc,)),
+        dma((plane_size,)),
+        dma((plane_size,)),
+        dma((zc,)),
+        dma((zc,)),
+    ]
+    operands = (tokens, routes, gates, saved, grad, gain, w_gate, w_up, w_down)
+    space = pltpu.MemorySpace.HBM
+    hbm = pl.BlockSpec(memory_space=space)
+    return pl.pallas_call(
+        functools.partial(fused_kernel, plane_size, slots),
+        out_shape=(
+            struct(tokens.shape, bf16),
+            struct(routes.shape, f32),
+            struct(w_gate.shape[1:], bf16),
+            struct(w_up.shape[1:], bf16),
+            struct(w_down.shape[1:], bf16),
+        ),
+        in_specs=[hbm] * 9,
+        out_specs=(vmem(),) * 5,
+        scratch_shapes=scratch + semaphores,
+        compiler_params=pltpu.CompilerParams(
+            collective_id=2, has_side_effects=True, vmem_limit_bytes=limit
+        ),
+        name="layer",
+    )(*(pltpu.with_memory_space_constraint(value, space) for value in operands))
+
+
+def size_of(refs):
+    total = 0
+    for ref in refs:
+        count = ref.dtype.itemsize if hasattr(ref.dtype, "itemsize") else jnp.dtype(ref.dtype).itemsize
+        for extent in ref.shape:
+            count *= extent
+        total += count
+    return total
+
+
+MIB = 1024 * 1024
+
+
+def put_kernel(*refs):
+    count = len(refs) // 2
+    copies = [pltpu.make_async_copy(refs[i], refs[count + i], refs[-1].at[i]) for i in range(count)]
+    for copy in copies:
+        copy.start()
+    for copy in copies:
+        copy.wait()
+
+
+def put_out(*values):
+    return pl.pallas_call(
+        put_kernel,
+        out_shape=tuple(jax.ShapeDtypeStruct(value.shape, value.dtype) for value in values),
+        in_specs=[vmem()] * len(values),
+        out_specs=(anywhere(),) * len(values),
+        scratch_shapes=[pltpu.SemaphoreType.DMA((len(values),))],
+        compiler_params=pltpu.CompilerParams(vmem_limit_bytes=MIB),
+        name="put",
+    )(*values)
+
+
+def local(tokens, routes, gates, w_gate, w_up, w_down, moe_out, norm_gain, out_grad):
+    z_count, x_count, t_count = (lax.axis_size(name) for name in AXES)
+    plane_size = x_count * t_count
+    tok_rows, features = tokens.shape
+    capacity = groups * tok_rows // (z_count * plane_size)
+    slots = -(-capacity // 16) * 16
+    group_rows = 3 * tok_rows // 8
+    scratch = fused_scratch(
+        tok_rows, features, moe_out.shape[1], w_gate.shape[2], group_rows, z_count, t_count, plane_size, slots
+    )
+    held = size_of(scratch)
+    grads = 3 * 2 * features * w_gate.shape[2]
+    if held + grads + 8 * MIB > 64 * MIB:
+        return apart(tokens, routes, gates, w_gate, w_up, w_down, moe_out, norm_gain, out_grad)
+    token_grad, rows, grad_gate, grad_up, grad_down = fused(
+        tokens,
+        routes.T,
+        gates.T,
+        moe_out,
+        out_grad,
+        norm_gain[None, :],
+        w_gate,
+        w_up,
+        w_down,
+        scratch,
+        held + 4 * MIB,
+        plane_size,
+        slots,
+        z_count,
+        t_count,
+    )
+    token_grad, gates_grad, grad_gate, grad_up, grad_down = put_out(
+        token_grad, rows.astype(jnp.bfloat16), grad_gate, grad_up, grad_down
+    )
+    return (token_grad, gates_grad.T, grad_gate[None], grad_up[None], grad_down[None])
+
+
 def solution(mesh):
     ep, tp = mesh.shape["ep"], mesh.shape["tp"]
     cut = Mesh(mesh.devices.reshape(groups, ep // groups, tp), AXES)

time: 142 us -> 94.8 us (0.67)
  matrix products: 37.1 us -> 0 us
  local copies, waits for them, and re-layouts: 6.59 us -> 0 us
  other arithmetic: 5.5 us -> 0.01 us
  Pallas kernels: 91.3 us -> 92.9 us
    dot_general x11 -> x0, matrix products: 37.1 us -> none  [the longest x8 25.6 us: contract(): lax.dot_general(left, right, (((left_dim,), (right_dim,)), ((), ())), pre...]
    unnamed x32 -> x0, local copies, waits for them, and re-layouts: 6.13 us -> none
    reduce_sum x3 -> x0, other arithmetic: 1.74 us -> none  [the longest x2 1.1 us: earlier_equal(): return jnp.sum(same.astype(jnp.int32), axis=-1)]
    pallas_call x2, Pallas kernels: 91.3 us -> 92.9 us  [the longest x1 88.9 us: fused(): pl.pallas_call(functools.partial(fused_kernel, plane_size, slots), out_sh...]
where the time goes in v2:
time: 94.8 us; the launch traced here: 93.5 us
  Pallas kernels  92.9 us (98%)
    pallas_call x1, Pallas kernels, fused(): pl.pallas_call(functools.partial(fused_kernel, plane_size, slots), out_sh...  88.9 us
    pallas_call x1, Pallas kernels, put_out(): pl.pallas_call(put_kernel, out_shape=tuple((jax.ShapeDtypeStruct(value.sh...  3.96 us

profile of v2, /device:TPU:0, one launch (start us, length us, event | category | flops | bytes accessed | tf_op | source)
XLA Modules:
  0.0 93.5 jit_solution(3520964809367728282)
XLA Ops:
  0.6 88.9 %layer.1 = (bf16[128,2048]{1,0:T(8,128)(2,1)S(1)}, f32[2,128]{1,0:T(2,128)S(1)}, bf16[2048,768]{1,0:T(8,128)(2,1)S(1)}, bf16[2048,768]{1,0:T(8,128)(2,1)S(1)}, bf16[768,2048]{1,0:T(8,128)(2,1)S(1)}) custom-call(bf16[128,2048]{1,0:T(8,128)(2,1)} %tok_hbm.1, s32[2,128]{1,0:T(2,128)} %bitcast.8, f32[2,128]{1,0:T(2,128)} %bitcast.9, bf16[512,512]{1,0:T(8,128)(2,1)} %saved_hbm.1, ...), custom_call_target="tpu_custom_call" | custom-call | tf_op jit(solution)/shard_map/layer/pallas_call | solution.py:938
  89.6 4.0 %put.1 = (bf16[128,2048]{1,0:T(8,128)(2,1)}, bf16[2,128]{1,0:T(2,128)(2,1)}, bf16[2048,768]{1,0:T(8,128)(2,1)}, bf16[2048,768]{1,0:T(8,128)(2,1)}, bf16[768,2048]{1,0:T(8,128)(2,1)}) custom-call(bf16[128,2048]{1,0:T(8,128)(2,1)S(1)} %get-tuple-element.15.refs_0_, bf16[2,128]{1,0:T(2,128)(2,1)S(1)} %convert_element_type.3.refs_1_, ...), custom_call_target="tpu_custom_call" | custom-call | tf_op jit(solution)/shard_map/put/pallas_call | solution.py:980
  (1 shorter events, 0.0 us)

commit v3 on v2

--- a/solution.py
+++ b/solution.py
@@ -69,8 +69,8 @@
     lax.fori_loop(first, last, lambda k, c: (act(k), c)[1], 0)
 
 
-def columns(features, act):
-    chunk = min(512, features)
+def columns(features, act, most=512):
+    chunk = min(most, features)
     each(0, features // chunk, lambda c: act(pl.ds(pl.multiple_of(c * chunk, chunk), chunk)))
 
 
@@ -534,8 +534,27 @@
         load.start()
     everyone = greet_all(place, True)
 
+    half, odd = z // (zc // 2), lax.rem(z, 2)
+
+    def apart_from(source):
+        return lax.rem(z - source + zc, zc)
+
+    near = apart_from(z + 1 - 2 * odd)
+    far = apart_from((zc - 1) * (1 - half))
+    late = apart_from(zc // 2 - half)
+    sending = [lax.rem(zc - d, zc) for d in (near, far, late)]
+    edge = half * odd + (1 - half) * (1 - odd)
+    early = edge * far + (1 - edge) * near
+    middle = edge * near + (1 - edge) * far
+
     def rows_of(q):
         return pl.ds(pl.multiple_of(q * slots, slots), slots)
+
+    def whole(d):
+        return pl.ds(pl.multiple_of(d * chunk, chunk), chunk)
+
+    def mine(d):
+        return isinstance(d, int) and d == 0
 
     def chunk_rows(d, q):
         return pl.ds(pl.multiple_of(d * chunk + q * slots, slots), slots)
@@ -583,7 +602,9 @@
         )
 
     def out_copy(d):
-        return remote(cbuf.at[d], land.at[z], os_sem.at[d], or_sem.at[d], place.back(d))
+        return remote(cbuf.at[d], land.at[own_land], os_sem.at[d], or_sem.at[d], place.back(d))
+
+    own_land = pl.ds(pl.multiple_of(z * group_rows, group_rows), group_rows)
 
     def gg_copy(k):
         q, device = peer(k)
@@ -599,10 +620,10 @@
         sel = picker(mbuf[d, t], chunk, group_rows)
 
         def one(cols):
-            rows = ztok[d, :, cols] if d else tokz[z, :, cols]
+            rows = tokz[z, :, cols] if mine(d) else ztok[d, :, cols]
             stok[d, :, cols] = jnp.dot(sel, rows, preferred_element_type=f32).astype(bf16)
 
-        columns(features, one)
+        columns(features, one, features)
         to_peers(lambda k: plane_copy(0, d, k))
         tok_in[chunk_rows(d, own), :] = stok[d, rows_of(own), :]
 
@@ -610,7 +631,7 @@
         for b in range(tc):
             sel = picker(mbuf[d, b], chunk, group_rows)
             rows = slice(b * group_rows, (b + 1) * group_rows)
-            value = zcot[d, rows, :] if d else cotz[z, rows, :]
+            value = cotz[z, rows, :] if mine(d) else zcot[d, rows, :]
             value = jnp.dot(sel, value, preferred_element_type=f32).astype(bf16)
             for q in range(plane_size):
                 scot[d, q, b * slots : (b + 1) * slots, :] = value[q * slots : (q + 1) * slots]
@@ -662,12 +683,12 @@
         for g in range(zc):
             tokz[g, :, cols] = value[g * group_rows : (g + 1) * group_rows]
 
-    columns(features, pack_tokens)
+    columns(features, pack_tokens, features)
     everyone()
 
     for d in range(zc):
         each(0 if d else 1, tc, lambda k: meta_copy(d, k).start())
-    for d in range(1, zc):
+    for d in sending:
         z_copy(0, d).start()
     mbuf[0, t] = meta[z]
 
@@ -703,7 +724,7 @@
         packed = jnp.dot(packer(mbuf[0, b, 4:5, :]), cot, preferred_element_type=f32).astype(bf16)
         for g in range(zc):
             cotz[g, b * group_rows : (b + 1) * group_rows, :] = packed[g * group_rows : (g + 1) * group_rows]
-    for d in range(1, zc):
+    for d in sending:
         z_copy(1, d).start()
     send_cot(0)
 
@@ -728,11 +749,11 @@
         return jnp.sum(jnp.where(iota(tile.shape, 1) == d, tile, 0.0), axis=1, keepdims=True)
 
     def compute(d):
-        rows = slice(d * chunk, (d + 1) * chunk)
+        rows = whole(d)
         for a in range(2):
             each(1, plane_size, lambda k: plane_copy(a, d, k).wait_recv())
         weight = weight_of(d)
-        step = 256
+        step = width
 
         def forward(c, total):
             cols = pl.ds(pl.multiple_of(c * step, step), step)
@@ -756,7 +777,7 @@
             back[d, :, cols] = value.astype(bf16)
             cot_in[rows, cols] = (weight * cot_in[rows, cols].astype(f32)).astype(bf16)
 
-        columns(features, backward)
+        columns(features, backward, features)
         return total
 
     def give_back(d):
@@ -769,13 +790,13 @@
 
         def one(cols):
             value = contract(sel, rbuf[d, :, cols], 0, 0).astype(bf16)
-            if d:
+            if mine(d):
+                land[own_land, cols] = value
+            else:
                 cbuf[d, :, cols] = value
-            else:
-                land[z, :, cols] = value
-
-        columns(features, one)
-        if d:
+
+        columns(features, one, features)
+        if not mine(d):
             out_copy(d).start()
 
     def weight_grad(out, left, right):
@@ -787,36 +808,38 @@
 
         each(0, out.shape[0] // step, one)
 
-    sums = [None] * zc
-    for d in range(1, zc):
-        z_copy(0, d).wait_recv()
-        send_tok(d)
-        if d == 1:
-            for load in loads[6:]:
-                load.wait()
-            each(1, plane_size, lambda k: w_copy(k).wait_recv())
-            sums[0] = compute(0)
-    for d in range(1, zc):
-        z_copy(1, d).wait_recv()
-        send_cot(d)
-    for d in range(1, zc):
-        sums[d] = compute(d)
-        if d < zc - 1:
-            give_back(d)
-    tile = jnp.zeros((chunk, LANES), f32)
-    for d in range(zc):
-        tile = jnp.where(iota((chunk, LANES), 1) == d, sums[d], tile)
+    def take(a, d):
+        z_copy(a, d).wait_recv()
+        if a == 0:
+            send_tok(d)
+        else:
+            send_cot(d)
+
+    def note(tile, d):
+        return jnp.where(iota((chunk, LANES), 1) == d, compute(d), tile)
+
+    take(0, early)
+    take(0, middle)
+    for load in loads[6:]:
+        load.wait()
+    each(1, plane_size, lambda k: w_copy(k).wait_recv())
+    tile = note(jnp.zeros((chunk, LANES), f32), 0)
+    take(1, early)
+    take(1, middle)
+    take(0, late)
+    tile = note(tile, early)
+    take(1, late)
+    tile = note(tile, middle)
+    give_back(far)
+    tile = note(tile, late)
     ggsend[...] = tile.astype(bf16)
     to_peers(gg_copy)
     ggbuf[rows_of(own)] = ggsend[rows_of(own)]
-    give_back(zc - 1)
+    give_back(late)
+    give_back(near)
     give_back(0)
-
-    grads = [(dwg_ref, tok_in, dg), (dwu_ref, tok_in, du), (dwd_ref, hid, cot_in)]
-    for d in range(1, zc):
-        unite(d)
-        if grads:
-            weight_grad(*grads.pop(0))
+    unite(far)
+    weight_grad(dwg_ref, tok_in, dg)
     each(1, plane_size, lambda k: gg_copy(k).wait_recv())
     returned = ggbuf[...].astype(f32)
     for d in range(zc):
@@ -827,20 +850,21 @@
         if d:
             gz_copy(d).start()
     gland[z] = gbuf[0]
-    unite(0)
-
+    unite(late)
+    weight_grad(dwu_ref, tok_in, du)
+    unite(near)
+    weight_grad(dwd_ref, hid, cot_in)
+    for d in range(zc):
+        each(0 if d else 1, tc, lambda k: meta_copy(d, k).wait_send())
+        for a in range(2):
+            each(1, plane_size, lambda k: plane_copy(a, d, k).wait_send())
+            if d:
+                z_copy(a, d).wait_send()
+    each(1, tc, lambda k: stat_copy(k).wait_send())
+    each(1, plane_size, lambda k: w_copy(k).wait_send())
+    each(1, plane_size, lambda k: gg_copy(k).wait_send())
     for d in range(1, zc):
         gz_copy(d).wait_recv()
-        out_copy(d).wait_recv()
-
-    def unpack(cols):
-        total = jnp.zeros((block, cols.size), f32)
-        for g in range(zc):
-            total = total + contract(own_pack[g * group_rows : (g + 1) * group_rows], land[g, :, cols], 0, 0)
-        tg_ref[:, cols] = total.astype(bf16)
-
-    columns(features, unpack)
-    slot_col = column(mbuf[0, t, 4:5, :])
     slot_row = mbuf[0, t, 4:5, :]
     for i in range(2):
         row = jnp.zeros((1, block), f32)
@@ -850,20 +874,19 @@
             hit = hit & (iota((block, block), 0) < group_rows)
             row = row + jnp.sum(jnp.where(hit, source, 0.0), axis=0, keepdims=True)
         gg_out[i : i + 1, :] = row
-
+    unite(0)
+    for d in range(1, zc):
+        out_copy(d).wait_recv()
+
+    def unpack(cols):
+        tg_ref[:, cols] = contract(own_pack, land[:, cols], 0, 0).astype(bf16)
+
+    columns(features, unpack, features)
     for d in range(zc):
-        each(0 if d else 1, tc, lambda k: meta_copy(d, k).wait_send())
-        for a in range(2):
-            each(1, plane_size, lambda k: plane_copy(a, d, k).wait_send())
-            if d:
-                z_copy(a, d).wait_send()
         each(1, plane_size, lambda k: return_copy(d, k).wait_send())
         if d:
             out_copy(d).wait_send()
             gz_copy(d).wait_send()
-    each(1, tc, lambda k: stat_copy(k).wait_send())
-    each(1, plane_size, lambda k: w_copy(k).wait_send())
-    each(1, plane_size, lambda k: gg_copy(k).wait_send())
 
 
 def fused_scratch(block, features, part, width, group_rows, zc, tc, plane_size, slots):
@@ -900,7 +923,7 @@
         space((zc, rows, features), bf16),
         space((zc, rows, features), bf16),
         space((zc, group_rows, features), bf16),
-        space((zc, group_rows, features), bf16),
+        space((zc * group_rows, features), bf16),
         space((rows, LANES), bf16),
         space((rows, LANES), bf16),
         space((zc,) + tile, f32),

time: 94.8 us -> 87.8 us (0.926); the launches traced: 93.5 us -> 87.6 us
  Pallas kernels: 92.9 us -> 86.8 us
    pallas_call x1, Pallas kernels: 88.9 us -> 82.8 us  [fused(): pl.pallas_call(functools.partial(fused_kernel, plane_size, slots), out_sh...]
where the time goes in v3:
time: 87.8 us; the launch traced here: 87.6 us
  Pallas kernels  86.8 us (99%)
    pallas_call x1, Pallas kernels, fused(): pl.pallas_call(functools.partial(fused_kernel, plane_size, slots), out_sh...  82.8 us
    pallas_call x1, Pallas kernels, put_out(): pl.pallas_call(put_kernel, out_shape=tuple((jax.ShapeDtypeStruct(value.sh...  3.96 us

profile of v3, /device:TPU:0, one launch (start us, length us, event | category | flops | bytes accessed | tf_op | source)
XLA Modules:
  0.0 87.6 jit_solution(740800310524247498)
XLA Ops:
  0.6 82.8 %layer.1 = (bf16[128,2048]{1,0:T(8,128)(2,1)S(1)}, f32[2,128]{1,0:T(2,128)S(1)}, bf16[2048,768]{1,0:T(8,128)(2,1)S(1)}, bf16[2048,768]{1,0:T(8,128)(2,1)S(1)}, bf16[768,2048]{1,0:T(8,128)(2,1)S(1)}) custom-call(bf16[128,2048]{1,0:T(8,128)(2,1)} %tok_hbm.1, s32[2,128]{1,0:T(2,128)} %bitcast.8, f32[2,128]{1,0:T(2,128)} %bitcast.9, bf16[512,512]{1,0:T(8,128)(2,1)} %saved_hbm.1, ...), custom_call_target="tpu_custom_call" | custom-call | tf_op jit(solution)/shard_map/layer/pallas_call | solution.py:961
  83.5 4.0 %put.1 = (bf16[128,2048]{1,0:T(8,128)(2,1)}, bf16[2,128]{1,0:T(2,128)(2,1)}, bf16[2048,768]{1,0:T(8,128)(2,1)}, bf16[2048,768]{1,0:T(8,128)(2,1)}, bf16[768,2048]{1,0:T(8,128)(2,1)}) custom-call(bf16[128,2048]{1,0:T(8,128)(2,1)S(1)} %get-tuple-element.15.refs_0_, bf16[2,128]{1,0:T(2,128)(2,1)S(1)} %convert_element_type.3.refs_1_, ...), custom_call_target="tpu_custom_call" | custom-call | tf_op jit(solution)/shard_map/put/pallas_call | solution.py:1003
  (1 shorter events, 0.0 us)

commit v4 on v3

--- a/solution.py
+++ b/solution.py
@@ -506,7 +506,15 @@
 ):
     place = Place(plane_size)
     z, x, t, zc, tc = place.z, place.x, place.t, place.zc, place.tc
-    own, peer = place.own, place.peer
+    own = place.own
+
+    def peer(k):
+        q, bit, rest = 0, 1, plane_size - k
+        while bit < plane_size:
+            flip = lax.rem(own // bit + rest // bit, 2)
+            q, bit = q + flip * bit, bit * 2
+        return q, (z, q // tc, lax.rem(q, tc))
+
     block, features = tok.shape
     part = saved_ref.shape[-1]
     group_rows = tokz.shape[1]
@@ -595,11 +603,15 @@
         q, device = peer(k)
         return remote(wsend.at[rows_of(q)], wrecv.at[rows_of(own)], ws_sem.at[k], wr_sem.at[k], device)
 
-    def return_copy(d, k):
+    def return_copy(d, k, piece=0):
         q, device = peer(k)
-        return remote(
-            back.at[d, rows_of(q)], rbuf.at[d, rows_of(own)], rs_sem.at[d, k], rr_sem.at[d, k], device
-        )
+        if mine(d):
+            cols = pl.ds(piece * (features // 2), features // 2)
+            src, dst = back.at[d, rows_of(q), cols], rbuf.at[d, rows_of(own), cols]
+        else:
+            src, dst = back.at[d, rows_of(q)], rbuf.at[d, rows_of(own)]
+        sem = zc if piece else d
+        return remote(src, dst, rs_sem.at[sem, k], rr_sem.at[sem, k], device)
 
     def out_copy(d):
         return remote(cbuf.at[d], land.at[own_land], os_sem.at[d], or_sem.at[d], place.back(d))
@@ -750,27 +762,20 @@
 
     def compute(d):
         rows = whole(d)
-        for a in range(2):
-            each(1, plane_size, lambda k: plane_copy(a, d, k).wait_recv())
         weight = weight_of(d)
-        step = width
-
-        def forward(c, total):
-            cols = pl.ds(pl.multiple_of(c * step, step), step)
-            token = tok_in[rows, :]
-            pre_gate = jnp.dot(token, wg[:, cols], preferred_element_type=f32)
-            pre_up = jnp.dot(token, wu[:, cols], preferred_element_type=f32)
-            hid_grad = contract(cot_in[rows, :], wd[cols, :], 1, 1)
-            sigmoid = jax.nn.sigmoid(pre_gate)
-            activated = pre_gate * sigmoid
-            hidden = activated * pre_up
-            d_hidden = weight * hid_grad
-            hid[rows, cols] = hidden.astype(bf16)
-            dg[rows, cols] = (d_hidden * pre_up * sigmoid * (1.0 + pre_gate * (1.0 - sigmoid))).astype(bf16)
-            du[rows, cols] = (d_hidden * activated).astype(bf16)
-            return total + jnp.sum(hidden * hid_grad, axis=1, keepdims=True)
-
-        total = lax.fori_loop(0, width // step, forward, jnp.zeros((chunk, 1), f32))
+        each(1, plane_size, lambda k: plane_copy(0, d, k).wait_recv())
+        pre_gate = jnp.dot(tok_in[rows, :], wg[...], preferred_element_type=f32)
+        pre_up = jnp.dot(tok_in[rows, :], wu[...], preferred_element_type=f32)
+        each(1, plane_size, lambda k: plane_copy(1, d, k).wait_recv())
+        hid_grad = contract(cot_in[rows, :], wd[...], 1, 1)
+        sigmoid = jax.nn.sigmoid(pre_gate)
+        activated = pre_gate * sigmoid
+        hidden = activated * pre_up
+        d_hidden = weight * hid_grad
+        hid[rows, :] = hidden.astype(bf16)
+        dg[rows, :] = (d_hidden * pre_up * sigmoid * (1.0 + pre_gate * (1.0 - sigmoid))).astype(bf16)
+        du[rows, :] = (d_hidden * activated).astype(bf16)
+        total = jnp.sum(hidden * hid_grad, axis=1, keepdims=True)
 
         def backward(cols):
             value = contract(dg[rows, :], wg[cols, :], 1, 1) + contract(du[rows, :], wu[cols, :], 1, 1)
@@ -780,12 +785,14 @@
         columns(features, backward, features)
         return total
 
-    def give_back(d):
-        to_peers(lambda k: return_copy(d, k))
+    def give_back(d, piece=0):
+        to_peers(lambda k: return_copy(d, k, piece))
         rbuf[d, rows_of(own)] = back[d, rows_of(own)]
 
     def unite(d):
         each(1, plane_size, lambda k: return_copy(d, k).wait_recv())
+        if mine(d):
+            each(1, plane_size, lambda k: return_copy(d, k, 1).wait_recv())
         sel = picker(mbuf[d, t], chunk, group_rows)
 
         def one(cols):
@@ -838,6 +845,7 @@
     give_back(late)
     give_back(near)
     give_back(0)
+    give_back(0, 1)
     unite(far)
     weight_grad(dwg_ref, tok_in, dg)
     each(1, plane_size, lambda k: gg_copy(k).wait_recv())
@@ -866,6 +874,7 @@
     for d in range(1, zc):
         gz_copy(d).wait_recv()
     slot_row = mbuf[0, t, 4:5, :]
+    outs = []
     for i in range(2):
         row = jnp.zeros((1, block), f32)
         for g in range(zc):
@@ -873,7 +882,8 @@
             hit = iota((block, block), 0).astype(f32) + float(g * group_rows) == slot_row
             hit = hit & (iota((block, block), 0) < group_rows)
             row = row + jnp.sum(jnp.where(hit, source, 0.0), axis=0, keepdims=True)
-        gg_out[i : i + 1, :] = row
+        outs.append(row)
+    gg_out[...] = jnp.concatenate(outs).astype(bf16)
     unite(0)
     for d in range(1, zc):
         out_copy(d).wait_recv()
@@ -884,6 +894,8 @@
     columns(features, unpack, features)
     for d in range(zc):
         each(1, plane_size, lambda k: return_copy(d, k).wait_send())
+        if d == 0:
+            each(1, plane_size, lambda k: return_copy(d, k, 1).wait_send())
         if d:
             out_copy(d).wait_send()
             gz_copy(d).wait_send()
@@ -946,8 +958,8 @@
         dma((2, zc, plane_size)),
         dma((plane_size,)),
         dma((plane_size,)),
-        dma((zc, plane_size)),
-        dma((zc, plane_size)),
+        dma((zc + 1, plane_size)),
+        dma((zc + 1, plane_size)),
         dma((zc,)),
         dma((zc,)),
         dma((plane_size,)),
@@ -962,7 +974,7 @@
         functools.partial(fused_kernel, plane_size, slots),
         out_shape=(
             struct(tokens.shape, bf16),
-            struct(routes.shape, f32),
+            struct(routes.shape, bf16),
             struct(w_gate.shape[1:], bf16),
             struct(w_up.shape[1:], bf16),
             struct(w_down.shape[1:], bf16),
@@ -992,7 +1004,13 @@
 
 def put_kernel(*refs):
     count = len(refs) // 2
-    copies = [pltpu.make_async_copy(refs[i], refs[count + i], refs[-1].at[i]) for i in range(count)]
+    copies = []
+    for i in range(count):
+        rows = refs[i].shape[0]
+        pieces = 4 if rows % 64 == 0 else 1
+        for n in range(pieces):
+            part = slice(n * rows // pieces, (n + 1) * rows // pieces)
+            copies.append(pltpu.make_async_copy(refs[i].at[part], refs[count + i].at[part], refs[-1].at[i, n]))
     for copy in copies:
         copy.start()
     for copy in copies:
@@ -1005,7 +1023,7 @@
         out_shape=tuple(jax.ShapeDtypeStruct(value.shape, value.dtype) for value in values),
         in_specs=[vmem()] * len(values),
         out_specs=(anywhere(),) * len(values),
-        scratch_shapes=[pltpu.SemaphoreType.DMA((len(values),))],
+        scratch_shapes=[pltpu.SemaphoreType.DMA((len(values), 4))],
         compiler_params=pltpu.CompilerParams(vmem_limit_bytes=MIB),
         name="put",
     )(*values)
@@ -1043,7 +1061,7 @@
         t_count,
     )
     token_grad, gates_grad, grad_gate, grad_up, grad_down = put_out(
-        token_grad, rows.astype(jnp.bfloat16), grad_gate, grad_up, grad_down
+        token_grad, rows, grad_gate, grad_up, grad_down
     )
     return (token_grad, gates_grad.T, grad_gate[None], grad_up[None], grad_down[None])
 

time: 87.8 us -> 87 us (level)
  no operation moved by 1% of the time
where the time goes in v4:
time: 87 us; the launch traced here: 86.9 us
  Pallas kernels  86 us (99%)
    pallas_call x1, Pallas kernels, fused(): pl.pallas_call(functools.partial(fused_kernel, plane_size, slots), out_sh...  82.1 us
    pallas_call x1, Pallas kernels, put_out(): pl.pallas_call(put_kernel, out_shape=tuple((jax.ShapeDtypeStruct(value.sh...  3.95 us

profile of v4, /device:TPU:0, one launch (start us, length us, event | category | flops | bytes accessed | tf_op | source)
XLA Modules:
  0.0 86.9 jit_solution(3915049796712792281)
XLA Ops:
  0.6 82.1 %layer.1 = (bf16[128,2048]{1,0:T(8,128)(2,1)S(1)}, bf16[2,128]{1,0:T(2,128)(2,1)S(1)}, bf16[2048,768]{1,0:T(8,128)(2,1)S(1)}, bf16[2048,768]{1,0:T(8,128)(2,1)S(1)}, bf16[768,2048]{1,0:T(8,128)(2,1)S(1)}) custom-call(bf16[128,2048]{1,0:T(8,128)(2,1)} %tok_hbm.1, s32[2,128]{1,0:T(2,128)} %bitcast.8, f32[2,128]{1,0:T(2,128)} %bitcast.9, ...), custom_call_target="tpu_custom_call" | custom-call | tf_op jit(solution)/shard_map/layer/pallas_call | solution.py:973
  82.7 3.9 %put.1 = (bf16[128,2048]{1,0:T(8,128)(2,1)}, bf16[2,128]{1,0:T(2,128)(2,1)}, bf16[2048,768]{1,0:T(8,128)(2,1)}, bf16[2048,768]{1,0:T(8,128)(2,1)}, bf16[768,2048]{1,0:T(8,128)(2,1)}) custom-call(bf16[128,2048]{1,0:T(8,128)(2,1)S(1)} %get-tuple-element.15.refs_0_, bf16[2,128]{1,0:T(2,128)(2,1)S(1)} %get-tuple-element.16.refs_1_, ...), custom_call_target="tpu_custom_call" | custom-call | tf_op jit(solution)/shard_map/put/pallas_call | solution.py:1021
